TPU v7x, 512 devices: a whole 4x4x16 slice. The times are simulated.
512 devices in a mesh: sp: 64 (over z, y), tp: 8 (over x, core).
Axes of the slice: x: 4, y: 4, z: 16, core: 2. Of those that a mesh axis runs over, the one named last changes fastest.
Arguments:
- receptance: bfloat16 [12288, 1024], P('sp', 'tp'), may hold values from -6 to 6
- head_keys: bfloat16 [12288, 1024], P('sp', 'tp'), may hold values from -6 to 6
- head_values: bfloat16 [12288, 1024], P('sp', 'tp'), may hold values from -6 to 6
- decay_preact: float32 [12288, 1024], P('sp', 'tp'), may hold values from -13.5 to -0.5
- learning_rate_preact: float32 [12288, 1024], P('sp', 'tp'), may hold values from -10.5 to 2.5
- output_gate_preact: bfloat16 [12288, 1024], P('sp', 'tp'), may hold values from -8 to 8
- self_token_weight: float32 [16, 64], P('tp'), may hold values from -0.6 to 0.6
- head_norm_gain: float32 [1024], P('tp'), may hold values from 0.1 to 1.9
- output_weight: bfloat16 [1024, 2048], P('tp'), may hold values from -0.1875 to 0.1875
- residual: bfloat16 [12288, 2048], P('sp'), may hold values from -6 to 6
- premixer_norm_gain: float32 [2048], replicated, may hold values from 0.1 to 1.9
- mixer_gate_weight: bfloat16 [2048, 5120], P('sp', 'tp'), may hold values from -0.125 to 0.125
- mixer_up_weight: bfloat16 [2048, 5120], P('sp', 'tp'), may hold values from -0.125 to 0.125
- mixer_down_weight: bfloat16 [5120, 2048], P('tp', 'sp'), may hold values from -0.078125 to 0.078125
Outputs:
- layer_out: bfloat16 [12288, 2048], P(('sp', 'tp'))
All inputs are finite; a program needn't handle non-finite values.
Results may differ from a plain program's by a relative error of at most 0.015.
Values may be sent and summed in bfloat16 or wider, within the bound.
A program may use at most 64 MiB of HBM per device.

v0:
```python
import functools

import jax
import jax.numpy as jnp
from jax import lax
from jax.experimental import pallas as pl
from jax.experimental.pallas import tpu as pltpu
from jax.sharding import PartitionSpec as P

HEAD = 64
LANES = 2 * HEAD
GROUP_EPS = 0.00064
NORM_EPS = 1e-06
NN = (((1,), (0,)), ((), ()))
NT = (((1,), (1,)), ((), ()))
TN = (((0,), (0,)), ((), ()))
INNER = 4


def split(x):
    high = x.astype(jnp.bfloat16)
    return high, (x - high.astype(jnp.float32)).astype(jnp.bfloat16)


def dot1(a, b, dims=NN):
    return lax.dot_general(
        a.astype(jnp.bfloat16), b.astype(jnp.bfloat16), dims, preferred_element_type=jnp.float32
    )


def dot3(a, b, dims=NN):
    ah, al = a if isinstance(a, tuple) else split(a)
    bh, bl = b if isinstance(b, tuple) else split(b)
    d = functools.partial(
        lax.dot_general, dimension_numbers=dims, preferred_element_type=jnp.float32
    )
    return d(ah, bh) + (d(ah, bl) + d(al, bh))


def per_head_sum(x, first):
    s0 = jnp.sum(jnp.where(first, x, 0.0), axis=-1, keepdims=True)
    s1 = jnp.sum(jnp.where(first, 0.0, x), axis=-1, keepdims=True)
    return jnp.where(first, s0, s1)


def block_diag_mask():
    row = lax.broadcasted_iota(jnp.int32, (LANES, LANES), 0)
    col = lax.broadcasted_iota(jnp.int32, (LANES, LANES), 1)
    return row // HEAD == col // HEAD, row == col


def fold(full):
    mask, _ = block_diag_mask()
    kept = jnp.where(mask, full, 0.0)
    return kept[:HEAD] + kept[HEAD:]


def unfold(packed):
    mask, _ = block_diag_mask()
    return jnp.where(mask, jnp.concatenate([packed, packed], axis=0), 0.0)


def local_kernel(r_ref, k_ref, v_ref, dw_ref, lw_ref, q_ref, y_ref, ps_ref):
    steps = r_ref.shape[0]
    f32 = jnp.float32
    first = lax.broadcasted_iota(jnp.int32, (steps, LANES), 1) < HEAD
    row = lax.broadcasted_iota(jnp.int32, (steps, steps), 0)
    col = lax.broadcasted_iota(jnp.int32, (steps, steps), 1)
    r, k, v = (x[...].astype(f32) for x in (r_ref, k_ref, v_ref))
    log_decay = jax.nn.sigmoid(dw_ref[...]) * (-0.6065306597126334)
    ones = (row >= col).astype(jnp.bfloat16)
    h0 = log_decay.astype(jnp.bfloat16)
    rest = log_decay - h0.astype(f32)
    h1 = rest.astype(jnp.bfloat16)
    h2 = (rest - h1.astype(f32)).astype(jnp.bfloat16)
    total = dot1(ones, h0) + (dot1(ones, h1) + dot1(ones, h2))
    last = total[steps - 1 :, :]
    unit = k / jnp.maximum(jnp.sqrt(per_head_sum(k * k, first)), 1.0)
    insert = unit * jax.nn.sigmoid(lw_ref[...])
    undo = jnp.exp(-total)
    remaining = jnp.exp(last - total)
    a_bar = -unit * jnp.exp(total - log_decay)
    r_bar = r * jnp.exp(total)
    b_hat = insert * undo
    k_hat = k * undo
    right = split(jnp.concatenate([b_hat, k_hat], axis=0))
    left = jnp.concatenate([a_bar, r_bar], axis=0)
    first2 = jnp.concatenate([first, first], axis=0)
    grams = [
        dot3(jnp.where(first2 if h == 0 else ~first2, left, 0.0), right, NT) for h in (0, 1)
    ]
    strict, incl = row > col, row >= col
    ab = [jnp.where(strict, g[:steps, :steps], 0.0) for g in grams]
    ak = [jnp.where(strict, g[:steps, steps:], 0.0) for g in grams]
    rb = [jnp.where(incl, g[steps:, :steps], 0.0) for g in grams]
    rk = [jnp.where(incl, g[steps:, steps:], 0.0) for g in grams]
    vb = v_ref[...]

    def times_v(m):
        mh, ml = split(m)
        return dot1(mh, vb) + dot1(ml, vb)

    seeds = [jnp.concatenate([a_bar, times_v(m)], axis=1) for m in ak]
    ab16 = [m.astype(jnp.bfloat16) for m in ab]
    eye = (row == col).astype(f32)
    size = 1
    inv = None
    while size < steps:
        joined = (
            (row // (2 * size) == col // (2 * size))
            & ((row // size) % 2 == 1)
            & ((col // size) % 2 == 0)
        )
        parts = [jnp.where(joined, m, jnp.zeros_like(m)) for m in ab16]
        if inv is None:
            inv = [eye + p.astype(f32) for p in parts]
        else:
            t16 = [t.astype(jnp.bfloat16) for t in inv]
            mid = [dot1(t, p) for t, p in zip(t16, parts)]
            inv = [t + dot1(m, tt) for t, m, tt in zip(inv, mid, t16)]
        size *= 2
    inv16 = [t.astype(jnp.bfloat16) for t in inv]
    absp = [split(m) for m in ab]
    sol = [dot1(t, s) for t, s in zip(inv16, seeds)]
    for _ in range(2):
        res = [s - x + dot3(m, x) for s, x, m in zip(seeds, sol, absp)]
        sol = [x + dot1(t, e) for x, t, e in zip(sol, inv16, res)]
    outs = [dot3(m, x) for m, x in zip(rb, sol)]
    own = [times_v(m) for m in rk]
    q_ref[...] = r_bar + jnp.where(first, outs[0][:, :LANES], outs[1][:, :LANES])
    y_ref[...] = jnp.where(first, outs[0][:, LANES:] + own[0], outs[1][:, LANES:] + own[1])
    w = jnp.where(first, sol[0][:, :LANES], sol[1][:, :LANES])
    u = jnp.where(first, sol[0][:, LANES:], sol[1][:, LANES:])
    b_end = split(insert * remaining)
    _, diag = block_diag_mask()
    prod = dot3(w, b_end, TN) + jnp.where(diag, jnp.exp(last), 0.0)
    kh, kl = split(k * remaining)
    state = dot3(u, b_end, TN) + dot1(vb, kh, TN) + dot1(vb, kl, TN)
    ps_ref[0, 0] = fold(prod)
    ps_ref[0, 1] = fold(state)


def join_kernel(i_ref, ps_ref, q_ref, y_ref, r_ref, k_ref, v_ref, g_ref, tw_ref, hg_ref, w_ref, o_ref):
    steps = q_ref.shape[0]
    pairs = q_ref.shape[1] // LANES
    f32 = jnp.float32
    first = lax.broadcasted_iota(jnp.int32, (steps, LANES), 1) < HEAD

    def turn(j, states):
        return tuple(
            dot3(s, unfold(ps_ref[j, p, 0])) + unfold(ps_ref[j, p, 1])
            for p, s in enumerate(states)
        )

    zero = jnp.zeros((LANES, LANES), f32)
    states = lax.fori_loop(0, i_ref[0], turn, (zero,) * pairs)
    mixed = []
    for p in range(pairs):
        cut = slice(p * LANES, (p + 1) * LANES)
        y = dot3(q_ref[:, cut], states[p], NT) + y_ref[:, cut]
        y = y - per_head_sum(y, first) * (1.0 / HEAD)
        spread = per_head_sum(y * y, first) * (1.0 / HEAD)
        r, k, v = (x[:, cut].astype(f32) for x in (r_ref, k_ref, v_ref))
        own = per_head_sum(r * k * tw_ref[:, cut], first) * v
        out = y * lax.rsqrt(spread + GROUP_EPS) * hg_ref[:, cut] + own
        mixed.append((out * jax.nn.sigmoid(g_ref[:, cut].astype(f32))).astype(jnp.bfloat16))
    mixed = jnp.concatenate(mixed, axis=1)
    o_ref[...] = jnp.dot(mixed, w_ref[...], preferred_element_type=f32).astype(jnp.bfloat16)


def recurrence(r, k, v, dw, lw):
    steps, width = r.shape
    pairs = width // LANES
    cols = pl.BlockSpec((steps, LANES), lambda p: (0, p))
    return pl.pallas_call(
        local_kernel,
        grid=(pairs,),
        in_specs=[cols] * 5,
        out_specs=[cols, cols, pl.BlockSpec((1, 2, HEAD, LANES), lambda p: (p, 0, 0, 0))],
        out_shape=[
            jax.ShapeDtypeStruct((steps, width), jnp.float32),
            jax.ShapeDtypeStruct((steps, width), jnp.float32),
            jax.ShapeDtypeStruct((pairs, 2, HEAD, LANES), jnp.float32),
        ],
        cost_estimate=pl.CostEstimate(
            flops=20_000_000_000, bytes_accessed=4_000_000, transcendentals=1_000_000
        ),
        name="local_part",
    )(r, k, v, dw, lw)


def join(index, ps, q, y, r, k, v, gate, tw, hg, w):
    vmem = pl.BlockSpec(memory_space=pltpu.VMEM)
    return pl.pallas_call(
        join_kernel,
        in_specs=[pl.BlockSpec(memory_space=pltpu.SMEM)] + [vmem] * 10,
        out_specs=vmem,
        out_shape=jax.ShapeDtypeStruct((q.shape[0], w.shape[1]), jnp.bfloat16),
        cost_estimate=pl.CostEstimate(
            flops=10_000_000_000, bytes_accessed=8_000_000, transcendentals=100_000
        ),
        name="join_part",
    )(index, ps, q, y, r, k, v, gate, tw, hg, w)


def rms_scale(rows, gain):
    x = rows.astype(jnp.float32)
    factor = lax.rsqrt(jnp.mean(x * x, axis=-1, keepdims=True) + NORM_EPS)
    return (x * factor * gain[None]).astype(jnp.bfloat16)


def per_device(r, k, v, dw, lw, gate, tw, hg, w_out, residual, gain, w_gate, w_up, w_down):
    steps = r.shape[0]
    sp, tp = lax.axis_size("sp"), lax.axis_size("tp")
    inner = INNER if sp % INNER == 0 else 1
    near = [[g * inner + i for i in range(inner)] for g in range(sp // inner)]
    far = [[g * inner + i for g in range(sp // inner)] for i in range(inner)]
    hidden = w_gate.shape[1] // inner

    q, y, ps = recurrence(r, k, v, dw, lw)
    ps_all = lax.all_gather(ps, "sp")

    def by_columns(w):
        w = lax.all_to_all(
            w, "sp", split_axis=1, concat_axis=0, axis_index_groups=near, tiled=True
        )
        return lax.all_gather(w, "sp", axis_index_groups=far, axis=0, tiled=False)

    g_all, u_all = by_columns(w_gate), by_columns(w_up)
    g_all = g_all.reshape(-1, hidden)
    u_all = u_all.reshape(-1, hidden)
    d_part = lax.all_to_all(
        w_down, "sp", split_axis=0, concat_axis=1, axis_index_groups=near, tiled=True
    )
    d_all = lax.all_gather(d_part, "sp", axis_index_groups=far, axis=1, tiled=True)

    index = lax.axis_index("sp").astype(jnp.int32).reshape(1)
    part = join(
        index, ps_all, q, y, r, k, v, gate, tw.reshape(1, -1), hg.reshape(1, -1), w_out
    )
    own_rows = steps // tp
    start = lax.axis_index("tp") * own_rows
    mix = lax.all_to_all(part.reshape(tp, own_rows, -1), "tp", 0, 0)
    mix = jnp.sum(mix.astype(jnp.float32), axis=0).astype(jnp.bfloat16).astype(jnp.float32)
    mine = lax.dynamic_slice_in_dim(residual, start, own_rows, 0)
    after = (mine.astype(jnp.float32) + mix).astype(jnp.bfloat16)
    normed = lax.all_gather(rms_scale(after, gain), "tp", axis=0, tiled=True)
    normed = lax.all_gather(normed, "sp", axis_index_groups=near, axis=0, tiled=True)
    g = jnp.dot(normed, g_all, preferred_element_type=jnp.float32)
    u = jnp.dot(normed, u_all, preferred_element_type=jnp.float32)
    h = (jax.nn.silu(g) * u).astype(jnp.bfloat16)
    down = jnp.dot(h, d_all, preferred_element_type=jnp.float32).astype(jnp.bfloat16)
    down = down.reshape(inner, tp, own_rows, -1)
    down = lax.all_to_all(down, "sp", 0, 0, axis_index_groups=near)
    down = jnp.sum(down.astype(jnp.float32), axis=0).astype(jnp.bfloat16)
    down = lax.all_to_all(down, "tp", 0, 0)
    down = jnp.sum(down.astype(jnp.float32), axis=0)
    return (after.astype(jnp.float32) + down).astype(jnp.bfloat16)


def solution(mesh):
    split_both = P("sp", "tp")
    placed = (split_both,) * 6 + (
        P("tp", None),
        P("tp"),
        P("tp", None),
        P("sp", None),
        P(),
        split_both,
        split_both,
        P("tp", "sp"),
    )
    return jax.shard_map(
        per_device, mesh=mesh, in_specs=placed, out_specs=P(("sp", "tp"), None), check_vma=False
    )
```

profile of v0, /device:TPU:1, one launch (start us, length us, event | category | flops | bytes accessed | tf_op | source)
XLA Modules:
  0.0 392.2 jit_solution(7941027166301489637)
XLA Ops:
  6.5 6.0 %local_part.1 = (f32[192,128]{1,0:T(8,128)}, f32[192,128]{1,0:T(8,128)}, f32[1,2,64,128]{3,2,1,0:T(8,128)}) custom-call(bf16[192,128]{1,0:T(8,128)(2,1)} %r_ref.3, bf16[192,128]{1,0:T(8,128)(2,1)} %k_ref.3, bf16[192,128]{1,0:T(8,128)(2,1)} %v_ref.3, f32[192,128]{1,0:T(8,128)} %dw_ref.1, f32[192,128]{1,0:T(8,128)} %lw_ref.1), custom_call_target="tpu_custom_call" | custom-call | flops 20000000000 | bytes 4000000 | tf_op jit(solution)/shard_map/local_part/pallas_call | solution.py:175
  12.6 0.7 reshape.42.tw_ref
  13.3 141.7 %all-gather.6.cloned.1.call-done = f32[64,2,64,128]{3,2,1,0:T(8,128)} async-done(((f32[1,2,64,128]{3,2,1,0:T(8,128)}), f32[64,2,64,128]{3,2,1,0:T(8,128)}) %all-gather.6.cloned.1.call-update) | async-done | bytes 4194320 | tf_op jit(solution)/shard_map/all_gather | solution.py:221
  155.0 4.2 %join_part.1 = bf16[192,2048]{1,0:T(8,128)(2,1)} custom-call(s32[1]{0:T(128)} %bitcast.i_ref, f32[64,1,2,64,128]{4,3,2,1,0:T(8,128)} %bitcast.40, f32[192,128]{1,0:T(8,128)} %get-tuple-element.9.q_ref, f32[192,128]{1,0:T(8,128)} %get-tuple-element.10.y_ref, bf16[192,128]{1,0:T(8,128)(2,1)} %r_ref.3, bf16[192,128]{1,0:T(8,128)(2,1)} %k_ref.3, ...), custom_call_target="tpu_custom_call" | custom-call | flops 10000000000 | bytes 8000000 | tf_op jit(solution)/shard_map/join_part/pallas_call | solution.py:194
  159.2 14.1 %all-to-all-start = ((bf16[8,24,2048]{2,1,0:T(8,128)(2,1)}), bf16[8,24,2048]{2,1,0:T(8,128)(2,1)S(1)}, u32[]{:S(2)}, u32[]{:S(2)}) async-start(bf16[8,24,2048]{2,1,0:T(8,128)(2,1)} %bitcast.36), calls=%async_computation | async-start | bytes 1572864 | tf_op jit(solution)/shard_map/all_to_all | solution.py:243
  173.3 12.2 %all-to-all-done = bf16[8,24,2048]{2,1,0:T(8,128)(2,1)S(1)} async-done(((bf16[8,24,2048]{2,1,0:T(8,128)(2,1)}), bf16[8,24,2048]{2,1,0:T(8,128)(2,1)S(1)}, u32[]{:S(2)}, u32[]{:S(2)}) %all-to-all-start) | async-done | bytes 786464 | tf_op jit(solution)/shard_map/all_to_all | solution.py:243
  185.5 1.0 fusion.14
  186.7 15.3 %all_gather.29 = bf16[192,2048]{1,0:T(8,128)(2,1)} all-gather(bf16[24,2048]{1,0:T(8,128)(2,1)S(1)} %fusion.16), channel_id=1, replica_groups=mesh['sp'=64,'tp'=8] {'tp'}, dimensions={0}, use_global_device_ids=true | all-gather | bytes 884736 | tf_op jit(solution)/shard_map/all_gather | solution.py:247
  202.1 0.6 copy.30
  202.7 3.3 all-to-all-start.1
  206.8 3.7 all-to-all-done.1
  210.5 3.3 all-to-all-start.2
  213.9 0.6 copy.36
  214.6 3.6 all-to-all-done.2
  218.2 3.3 all-to-all-start.3
  221.6 38.8 %all_gather.34 = bf16[16,128,160]{1,2,0:T(8,128)(2,1)S(1)} all-gather(bf16[1,128,160]{1,2,0:T(8,128)(2,1)S(1)} %copy.34), channel_id=1, replica_groups={{0,32,64,96,128,160,192,224,256,288,320,352,384,416,448,480},{8,40,72,1..., dimensions={0}, use_global_device_ids=true | all-gather | bytes 696320 | tf_op jit(solution)/shard_map/all_gather | solution.py:227
  260.4 23.5 %all_gather.32 = bf16[16,128,160]{1,2,0:T(8,128)(2,1)S(1)} all-gather(bf16[1,128,160]{1,2,0:T(8,128)(2,1)S(1)} %copy.31), channel_id=1, replica_groups={{0,32,64,96,128,160,192,224,256,288,320,352,384,416,448,480},{8,40,72,1..., dimensions={0}, use_global_device_ids=true | all-gather | bytes 696320 | tf_op jit(solution)/shard_map/all_gather | solution.py:227
  284.0 26.1 %all_gather.35 = bf16[160,2048]{0,1:T(8,128)(2,1)S(1)} all-gather(bf16[160,128]{0,1:T(8,128)(2,1)S(1)} %bitcast.37), channel_id=1, replica_groups={{0,32,64,96,128,160,192,224,256,288,320,352,384,416,448,480},{8,40,72,1..., dimensions={1}, use_global_device_ids=true | all-gather | bytes 696320 | tf_op jit(solution)/shard_map/all_gather | solution.py:235
  310.1 3.1 fusion.5
  313.2 6.1 %convolution_convert_fusion = bf16[768,2048]{1,0:T(8,128)(2,1)} fusion(bf16[160,2048]{0,1:T(8,128)(2,1)S(1)} %all_gather.35, bf16[768,2048]{1,0:T(8,128)(2,1)} %all-gather.4.cloned.1.call-done, f32[768,160]{0,1:T(8,128)S(1)} %fusion.5, bf16[16,128,160]{1,2,0:T(8,128)(2,1)S(1)} %all_gather.34), kind=kOutput, calls=%fused_computation | convolution fusion | flops 1008943104 | bytes 8093696 | tf_op jit(solution)/shard_map/dot_general | solution.py:252
  319.2 25.3 %all_to_all.66 = bf16[4,8,24,2048]{3,2,1,0:T(8,128)(2,1)S(1)} all-to-all(bf16[4,8,24,2048]{3,2,1,0:T(8,128)(2,1)} %bitcast.35), channel_id=1, replica_groups={{0,8,16,24},{32,40,48,56},{64,72,80,88},{96,104,112,120},{128,136,144,1..., dimensions={0} | all-to-all | bytes 6291456 | tf_op jit(solution)/shard_map/all_to_all | solution.py:254
  344.5 1.7 reduce_sum.44
  346.2 38.4 %all_to_all.67 = bf16[8,24,2048]{2,1,0:T(8,128)(2,1)S(1)} all-to-all(bf16[8,24,2048]{2,1,0:T(8,128)(2,1)} %reduce_sum.44), channel_id=1, replica_groups=mesh['sp'=64,'tp'=8] {'tp'}, dimensions={0} | all-to-all | bytes 1572864 | tf_op jit(solution)/shard_map/all_to_all | solution.py:256
  384.7 0.7 fusion.17
  (26 shorter events, 1.5 us)
Async XLA Ops:
  6.5 6.1 %copy-start.4 = (f32[2,64]{1,0:T(2,128)S(1)}, f32[2,64]{1,0:T(2,128)}, u32[]{:S(2)}) copy-start(f32[2,64]{1,0:T(2,128)} %param.20) | copy-start | bytes 1540
  6.5 148.5 %all-gather.6.cloned.1.call-start = ((), (), s32[]{:S(2)}) async-start(), calls=%async_computation.7 | async-start | bytes 4259840 | tf_op jit(solution)/shard_map/all_gather | solution.py:221
  155.0 31.6 %copy-start.3 = (f32[2048]{0:T(1024)S(1)}, f32[2048]{0:T(1024)}, u32[]{:S(2)}) copy-start(f32[2048]{0:T(1024)} %param.24) | copy-start | bytes 24580
  159.2 42.8 %copy-start = (bf16[32,640]{1,0:T(8,128)(2,1)S(1)}, bf16[32,640]{1,0:T(8,128)(2,1)}, u32[]{:S(2)}) copy-start(bf16[32,640]{1,0:T(8,128)(2,1)} %param.25) | copy-start | bytes 122884
  159.2 46.9 %copy-start.1 = (bf16[32,640]{1,0:T(8,128)(2,1)S(1)}, bf16[32,640]{1,0:T(8,128)(2,1)}, u32[]{:S(2)}) copy-start(bf16[32,640]{1,0:T(8,128)(2,1)} %param.26) | copy-start | bytes 122884
  159.2 54.6 %copy-start.2 = (bf16[640,32]{0,1:T(8,128)(2,1)S(1)}, bf16[640,32]{0,1:T(8,128)(2,1)}, u32[]{:S(2)}) copy-start(bf16[640,32]{0,1:T(8,128)(2,1)} %param.27) | copy-start | bytes 122884
  159.2 26.2 %all-to-all-start = ((bf16[8,24,2048]{2,1,0:T(8,128)(2,1)}), bf16[8,24,2048]{2,1,0:T(8,128)(2,1)S(1)}, u32[]{:S(2)}, u32[]{:S(2)}) async-start(bf16[8,24,2048]{2,1,0:T(8,128)(2,1)} %bitcast.36), calls=%async_computation | async-start | bytes 1572864 | tf_op jit(solution)/shard_map/all_to_all | solution.py:243
  173.3 136.8 %all-gather.4.cloned.1.call-start = ((), (), s32[]{:S(2)}) async-start(), calls=%async_computation.6 | async-start | bytes 3932160 | tf_op jit(solution)/shard_map/all_gather | solution.py:248
  202.7 7.7 %all-to-all-start.1 = ((bf16[32,4,160]{2,0,1:T(8,128)(2,1)}), bf16[32,4,160]{2,0,1:T(8,128)(2,1)S(1)}, u32[]{:S(2)}, u32[]{:S(2)}) async-start(bf16[32,4,160]{2,0,1:T(8,128)(2,1)} %copy.30), calls=%async_computation.1 | async-start | bytes 131072 | tf_op jit(solution)/shard_map/all_to_all | solution.py:224
  210.5 7.7 %all-to-all-start.2 = ((bf16[32,4,160]{2,0,1:T(8,128)(2,1)}), bf16[32,4,160]{2,0,1:T(8,128)(2,1)S(1)}, u32[]{:S(2)}, u32[]{:S(2)}) async-start(bf16[32,4,160]{2,0,1:T(8,128)(2,1)} %copy.33), calls=%async_computation.2 | async-start | bytes 131072 | tf_op jit(solution)/shard_map/all_to_all | solution.py:224
  218.2 65.8 %all-to-all-start.3 = ((bf16[4,160,32]{1,2,0:T(8,128)(2,1)}), bf16[4,160,32]{1,2,0:T(8,128)(2,1)S(1)}, u32[]{:S(2)}, u32[]{:S(2)}) async-start(bf16[4,160,32]{1,2,0:T(8,128)(2,1)} %copy.36), calls=%async_computation.3 | async-start | bytes 131072 | tf_op jit(solution)/shard_map/all_to_all | solution.py:232
Sparse Core Ops, SparseCore 0:
  12.7 142.2 all-gather.5
  202.1 48.0 all-gather.3
where the time goes:
time: 393 us; the launch traced here: 392 us
  blocking collectives  167 us (42%)
  waiting for transfers between devices  161 us (41%)
  starting transfers between devices  23.9 us (6%)
  between operations  13.5 us (3%)
  Pallas kernels  10.2 us (3%)
  matrix products  9.16 us (2%)
    all_gather x1, waiting for transfers between devices, per_device(): ps_all = lax.all_gather(ps, 'sp')  142 us
    all_gather x2, blocking collectives, by_columns(): return lax.all_gather(w, 'sp', axis_index_groups=far, axis=0, tiled=False)  62.3 us
    all_to_all x1, blocking collectives, per_device(): down = lax.all_to_all(down, 'tp', 0, 0)  38.4 us
    all_gather x1, blocking collectives, per_device(): lax.all_gather(d_part, 'sp', axis_index_groups=far, axis=1, tiled=True)  26.1 us
    all_to_all x1, blocking collectives, per_device(): down = lax.all_to_all(down, 'sp', 0, 0, axis_index_groups=near)  25.3 us
    all_gather x1, blocking collectives, per_device(): normed = lax.all_gather(rms_scale(after, gain), 'tp', axis=0, tiled=True)  15.3 us
    all_to_all x1, starting transfers between devices, per_device(): mix = lax.all_to_all(part.reshape(tp, own_rows, -1), 'tp', 0, 0)  14.1 us
    all_to_all x1, waiting for transfers between devices, per_device(): mix = lax.all_to_all(part.reshape(tp, own_rows, -1), 'tp', 0, 0)  12.2 us
  transfers between devices with their start and end apart: 6, of which 4 were waited for; matrix products, arithmetic and copies ran while one was open for 1% of the time, Pallas kernels for 0%

commit v1 on v0

v1 whole, which is shorter than its diff:
```python
import functools

import jax
import jax.numpy as jnp
from jax import lax
from jax.experimental import pallas as pl
from jax.experimental.pallas import tpu as pltpu
from jax.sharding import PartitionSpec as P

HEAD = 64
LANES = 2 * HEAD
GROUP_EPS = 0.00064
NORM_EPS = 1e-06
NN = (((1,), (0,)), ((), ()))
NT = (((1,), (1,)), ((), ()))
TN = (((0,), (0,)), ((), ()))
NX, NY, NZ, NC = 4, 4, 16, 2
NTP = NX * NC
NG = 4
HOPS = NZ // 2
MESH = pl.DeviceIdType.MESH
PACKET = LANES + 16


def split(x):
    high = x.astype(jnp.bfloat16)
    return high, (x - high.astype(jnp.float32)).astype(jnp.bfloat16)


def dot1(a, b, dims=NN):
    return lax.dot_general(
        a.astype(jnp.bfloat16), b.astype(jnp.bfloat16), dims, preferred_element_type=jnp.float32
    )


def dot3(a, b, dims=NN):
    ah, al = a if isinstance(a, tuple) else split(a)
    bh, bl = b if isinstance(b, tuple) else split(b)
    d = functools.partial(
        lax.dot_general, dimension_numbers=dims, preferred_element_type=jnp.float32
    )
    return d(ah, bh) + (d(ah, bl) + d(al, bh))


def per_head_sum(x, first):
    s0 = jnp.sum(jnp.where(first, x, 0.0), axis=-1, keepdims=True)
    s1 = jnp.sum(jnp.where(first, 0.0, x), axis=-1, keepdims=True)
    return jnp.where(first, s0, s1)


def block_diag_mask():
    row = lax.broadcasted_iota(jnp.int32, (LANES, LANES), 0)
    col = lax.broadcasted_iota(jnp.int32, (LANES, LANES), 1)
    return row // HEAD == col // HEAD


def fold(full):
    kept = jnp.where(block_diag_mask(), full, 0.0)
    return kept[:HEAD] + kept[HEAD:]


def unfold(packed):
    return jnp.where(block_diag_mask(), jnp.concatenate([packed, packed], axis=0), 0.0)


def fold_diag(d):
    row = lax.broadcasted_iota(jnp.int32, (HEAD, LANES), 0)
    col = lax.broadcasted_iota(jnp.int32, (HEAD, LANES), 1)
    return jnp.where(col % HEAD == row, d, 0.0)


def compose(a, b):
    both = dot3(jnp.concatenate([a[0], a[1]], axis=0), unfold(b[0]))
    return both[:HEAD], both[HEAD:] + b[1]


def put_packet(ref, slot, prod, state, decay):
    high, low = split(decay)
    row = lax.broadcasted_iota(jnp.int32, (16, LANES), 0)
    high, low = high.astype(jnp.float32), low.astype(jnp.float32)
    tail = jnp.where(row == 0, high, jnp.where(row == 1, low, 0.0))
    ref[slot, :HEAD, :] = (prod - fold_diag(decay)).astype(jnp.bfloat16)
    ref[slot, HEAD:LANES, :] = state.astype(jnp.bfloat16)
    ref[slot, LANES:, :] = tail.astype(jnp.bfloat16)


def get_packet(ref, slot):
    f32 = jnp.float32
    tail = ref[slot, LANES:, :].astype(f32)
    decay = tail[0:1] + tail[1:2]
    prod = ref[slot, :HEAD, :].astype(f32) + fold_diag(decay)
    return prod, ref[slot, HEAD:LANES, :].astype(f32), decay


def local_part(r_ref, k_ref, v_ref, dw_ref, lw_ref):
    steps = r_ref.shape[0]
    f32 = jnp.float32
    first = lax.broadcasted_iota(jnp.int32, (steps, LANES), 1) < HEAD
    row = lax.broadcasted_iota(jnp.int32, (steps, steps), 0)
    col = lax.broadcasted_iota(jnp.int32, (steps, steps), 1)
    r, k, v = (x[...].astype(f32) for x in (r_ref, k_ref, v_ref))
    log_decay = jax.nn.sigmoid(dw_ref[...]) * (-0.6065306597126334)
    ones = (row >= col).astype(jnp.bfloat16)
    h0 = log_decay.astype(jnp.bfloat16)
    rest = log_decay - h0.astype(f32)
    h1 = rest.astype(jnp.bfloat16)
    h2 = (rest - h1.astype(f32)).astype(jnp.bfloat16)
    total = dot1(ones, h0) + (dot1(ones, h1) + dot1(ones, h2))
    last = total[steps - 1 :, :]
    unit = k / jnp.maximum(jnp.sqrt(per_head_sum(k * k, first)), 1.0)
    insert = unit * jax.nn.sigmoid(lw_ref[...])
    undo = jnp.exp(-total)
    remaining = jnp.exp(last - total)
    a_bar = -unit * jnp.exp(total - log_decay)
    r_bar = r * jnp.exp(total)
    b_hat = insert * undo
    k_hat = k * undo
    right = split(jnp.concatenate([b_hat, k_hat], axis=0))
    left = jnp.concatenate([a_bar, r_bar], axis=0)
    first2 = jnp.concatenate([first, first], axis=0)
    grams = [
        dot3(jnp.where(first2 if h == 0 else ~first2, left, 0.0), right, NT) for h in (0, 1)
    ]
    strict, incl = row > col, row >= col
    ab = [jnp.where(strict, g[:steps, :steps], 0.0) for g in grams]
    ak = [jnp.where(strict, g[:steps, steps:], 0.0) for g in grams]
    rb = [jnp.where(incl, g[steps:, :steps], 0.0) for g in grams]
    rk = [jnp.where(incl, g[steps:, steps:], 0.0) for g in grams]
    vb = v_ref[...]

    def times_v(m):
        mh, ml = split(m)
        return dot1(mh, vb) + dot1(ml, vb)

    seeds = [jnp.concatenate([a_bar, times_v(m)], axis=1) for m in ak]
    ab16 = [m.astype(jnp.bfloat16) for m in ab]
    eye = (row == col).astype(f32)
    size = 1
    inv = None
    while size < steps:
        joined = (
            (row // (2 * size) == col // (2 * size))
            & ((row // size) % 2 == 1)
            & ((col // size) % 2 == 0)
        )
        parts = [jnp.where(joined, m, jnp.zeros_like(m)) for m in ab16]
        if inv is None:
            inv = [eye + p.astype(f32) for p in parts]
        else:
            t16 = [t.astype(jnp.bfloat16) for t in inv]
            mid = [dot1(t, p) for t, p in zip(t16, parts)]
            inv = [t + dot1(m, tt) for t, m, tt in zip(inv, mid, t16)]
        size *= 2
    inv16 = [t.astype(jnp.bfloat16) for t in inv]
    absp = [split(m) for m in ab]
    sol = [dot1(t, s) for t, s in zip(inv16, seeds)]
    for _ in range(2):
        res = [s - x + dot3(m, x) for s, x, m in zip(seeds, sol, absp)]
        sol = [x + dot1(t, e) for x, t, e in zip(sol, inv16, res)]
    w = jnp.where(first, sol[0][:, :LANES], sol[1][:, :LANES])
    u = jnp.where(first, sol[0][:, LANES:], sol[1][:, LANES:])
    b_end = split(insert * remaining)
    decay = jnp.exp(last)
    prod = fold(dot3(w, b_end, TN)) + fold_diag(decay)
    kh, kl = split(k * remaining)
    state = fold(dot3(u, b_end, TN) + dot1(vb, kh, TN) + dot1(vb, kl, TN))

    def outputs():
        outs = [dot3(m, x) for m, x in zip(rb, sol)]
        own = [times_v(m) for m in rk]
        q = r_bar + jnp.where(first, outs[0][:, :LANES], outs[1][:, :LANES])
        y = jnp.where(first, outs[0][:, LANES:] + own[0], outs[1][:, LANES:] + own[1])
        return q, y

    return prod, state, decay, outputs


def layer_kernel(
    r_ref, k_ref, v_ref, dw_ref, lw_ref, gate_ref, tw_ref, hg_ref, wg_ref, wu_ref, wd_ref,
    gain_ref, wo_hbm, res_hbm,
    out_ref,
    wall, wo, mixed, resid, after, normed, hid, parts, pair_in, pair_sum, last_in,
    ybuf, zbuf, gbuf, q_s, y_s, ent,
    send, r_wo, r_za, r_zb, r_ya, r_yf, r_yb, r_l1, r_l2, r_l3, r_mx, r_pair, r_last, loc,
):
    f32, bf16 = jnp.float32, jnp.bfloat16
    steps = r_ref.shape[0]
    depth, ff = wg_ref.shape
    plane = NY * depth
    half, phalf = depth // 2, plane // 2
    ca = 2 * ff
    model = wo.shape[1]
    own_rows = out_ref.shape[0]
    sp, tp = lax.axis_index("sp"), lax.axis_index("tp")
    z, y = sp // NY, sp % NY
    x, c = tp // NC, tp % NC
    zg, zl = z // NG, z % NG

    def dev(zz=None, yy=None, tt=None):
        zz = z if zz is None else zz
        yy = y if yy is None else yy
        return (zz * NY + yy, tp if tt is None else tt)

    def rcopy(src, dst, s, r, device):
        return pltpu.make_async_remote_copy(
            src_ref=src, dst_ref=dst, send_sem=s, recv_sem=r, device_id=device, device_id_type=MESH
        )

    def wait_bytes(ref, sem):
        pltpu.make_async_copy(ref, ref, sem).wait()

    up, down = (z + 1) % NZ, (z + NZ - 1) % NZ
    others_y = [dev(yy=(y + d) % NY) for d in range(1, NY)]
    others_zl = [dev(zz=zg * NG + (zl + d) % NG) for d in range(1, NG)]
    others_zg = [dev(zz=((zg + d) % NG) * NG + zl) for d in range(1, NG)]
    others_tp = [dev(tt=(tp + d) % NTP) for d in range(1, NTP)]
    ring = [dev(zz=up), dev(zz=down)]

    barrier = pltpu.get_barrier_semaphore()
    greet = others_y + others_zl + others_zg + others_tp + ring
    for d in greet:
        pl.semaphore_signal(barrier, inc=1, device_id=d, device_id_type=MESH)

    res_copy = pltpu.make_async_copy(res_hbm, resid, loc.at[0])
    res_copy.start()
    wo_rows = lambda t: wo.at[pl.ds(pl.multiple_of(t * LANES, LANES), LANES), :]
    wo_own = pltpu.make_async_copy(wo_hbm, wo_rows(tp), loc.at[1])
    wo_own.start()
    my_row = pl.multiple_of(sp * depth, depth)
    wall[pl.ds(my_row, depth), 0:ff] = wg_ref[...]
    wall[pl.ds(my_row, depth), ff:ca] = wu_ref[...]
    eye = (
        lax.broadcasted_iota(jnp.int32, (depth, depth), 0)
        == lax.broadcasted_iota(jnp.int32, (depth, depth), 1)
    ).astype(bf16)
    wall[pl.ds(my_row, depth), ca:] = dot1(eye, wd_ref[...], NT).astype(bf16)

    def rows(zz, yy, lo=0, n=None):
        return pl.ds(pl.multiple_of(zz * plane + yy * depth + lo, half), depth if n is None else n)

    def a_block(zz, yy, lo=0, n=None):
        return wall.at[rows(zz, yy, lo, n), 0:ca]

    def b_slab(zz, lo=0, n=None):
        n = plane if n is None else n
        return wall.at[pl.ds(pl.multiple_of(zz * plane + lo, phalf), n), ca:]

    def za(s):
        out = []
        for dirn in (0, 1):
            zz = (z + NZ - s) % NZ if dirn == 0 else (z + s) % NZ
            ref = a_block(zz, y) if s < HOPS - 1 else a_block(zz, y, half * dirn, half)
            out.append(rcopy(ref, ref, send.at[0], r_za.at[dirn, s], ring[dirn]))
        return out

    def zb(s):
        out = []
        for dirn in (0, 1):
            zz = (z + NZ - s) % NZ if dirn == 0 else (z + s) % NZ
            ref = b_slab(zz) if s < HOPS - 1 else b_slab(zz, phalf * dirn, phalf)
            out.append(rcopy(ref, ref, send.at[1], r_zb.at[dirn, s], ring[dirn]))
        return out

    def plane_of(i):
        if i == 0:
            return z
        s, dirn = (i - 1) // 2, (i - 1) % 2
        return (z + NZ - 1 - s) % NZ if dirn == 0 else (z + 1 + s) % NZ

    side = [dev(yy=(y + 1) % NY), dev(yy=(y + NY - 1) % NY)]

    def ya(i):
        ref = a_block(plane_of(i), y)
        return [rcopy(ref, ref, send.at[2], r_ya.at[d, i], side[d]) for d in (0, 1)]

    def yf(i):
        out = []
        for d in (0, 1):
            ref = a_block(plane_of(i), (y + NY - 1) % NY if d == 0 else (y + 1) % NY, half * d, half)
            out.append(rcopy(ref, ref, send.at[3], r_yf.at[0], side[d]))
        return out

    def start(copies):
        for cp in copies:
            cp.start()

    def wait_recv(copies):
        for cp in copies:
            cp.wait_recv()

    def yb():
        ref = wall.at[rows(z, y), ca:]
        return [rcopy(ref, ref, send.at[4], r_yb.at[d], others_y[d]) for d in range(NY - 1)]

    def exchange(buf, slot, sem, s, targets):
        return [
            rcopy(buf.at[slot], buf.at[slot], send.at[s], sem.at[d], t)
            for d, t in enumerate(targets)
        ]

    def wo_same(d):
        t = ((x + d) % NX) * NC + c
        return rcopy(wo_hbm, wo_rows(tp), send.at[5], r_wo.at[d - 1], dev(tt=t))

    partner = dev(tt=x * NC + 1 - c)

    def wo_relay(d):
        ref = wo_rows(((x + NX - d) % NX) * NC + c)
        return rcopy(ref, ref, send.at[6], r_wo.at[NX - 1], partner)

    pl.semaphore_wait(barrier, len(greet))

    for d in range(1, NX):
        wo_same(d).start()
    start(yb())
    start(za(0))
    start(ya(0))

    work = []

    def job(f, *a):
        work.append(functools.partial(f, *a))

    def b_open():
        wait_recv(yb())
        start(zb(0))

    def a_step(s):
        wait_recv(za(s))
        if s < HOPS - 1:
            start(za(s + 1))
        for i in [2 * s + 1, 2 * s + 2] if s < HOPS - 1 else [2 * s + 1]:
            start(ya(i))

    def b_step(s):
        wait_recv(zb(s))
        if s < HOPS - 1:
            start(zb(s + 1))

    def f_step(s):
        for i in [0] if s < 0 else [2 * s + 1, 2 * s + 2] if s < HOPS - 1 else [2 * s + 1]:
            wait_recv(ya(i))
            start(yf(i))

    job(b_open)
    job(f_step, -1)
    for s in range(HOPS):
        job(a_step, s)
        job(b_step, s)
        job(f_step, s)

    def serve(n):
        for _ in range(min(n, len(work))):
            work.pop(0)()

    prod, state, decay, outputs = local_part(r_ref, k_ref, v_ref, dw_ref, lw_ref)
    put_packet(ybuf, y, prod, state, decay)
    l1 = exchange(ybuf, y, r_l1, 7, others_y)
    start(l1)
    q, y_own = outputs()
    q_s[...] = q
    y_s[...] = y_own
    wo_own.wait()
    wo_relay(0).start()
    serve(SERVE[0])
    wait_recv(l1)

    def total(buf):
        m = [get_packet(buf, j) for j in range(4)]
        ab, cd = compose(m[0], m[1]), compose(m[2], m[3])
        return (*compose(ab, cd), (m[0][2] * m[1][2]) * (m[2][2] * m[3][2]))

    put_packet(zbuf, zl, *total(ybuf))
    l2 = exchange(zbuf, zl, r_l2, 8, others_zl)
    start(l2)
    serve(SERVE[1])
    wait_recv(l2)
    put_packet(gbuf, zg, *total(zbuf))
    l3 = exchange(gbuf, zg, r_l3, 9, others_zg)
    for d in range(1, NG):
        @pl.when(zg + d < NG)
        def _(d=d):
            l3[d - 1].start()

    def before(buf, count, begin):
        ent[...] = jnp.concatenate(begin, axis=0)

        def step(j, _):
            p, u, _ = get_packet(buf, j)
            both = dot3(ent[...], unfold(p))
            ent[0:HEAD, :] = both[:HEAD]
            ent[HEAD:, :] = both[HEAD:] + u
            return 0

        lax.fori_loop(0, count, step, 0)
        return ent[0:HEAD, :], ent[HEAD:, :]

    ident = (fold_diag(jnp.ones((1, LANES), f32)), jnp.zeros((HEAD, LANES), f32))
    entry = before(ybuf, y, before(zbuf, zl, ident))
    for d in range(1, NX):
        wo_same(d).wait_recv()
        wo_relay(d).start()
    serve(SERVE[2])
    for d in range(1, NG):
        @pl.when(zg >= d)
        def _(d=d):
            l3[d - 1].wait_recv()

    def turn(j, s):
        p, u, _ = get_packet(gbuf, j)
        return dot3(s, unfold(p)) + u

    s_in = lax.fori_loop(0, zg, turn, jnp.zeros((HEAD, LANES), f32))
    s_in = dot3(s_in, unfold(entry[0])) + entry[1]

    first = lax.broadcasted_iota(jnp.int32, (steps, LANES), 1) < HEAD
    yy = dot3(q_s[...], unfold(s_in), NT) + y_s[...]
    yy = yy - per_head_sum(yy, first) * (1.0 / HEAD)
    spread = per_head_sum(yy * yy, first) * (1.0 / HEAD)
    r, k, v = (a[...].astype(f32) for a in (r_ref, k_ref, v_ref))
    own = per_head_sum(r * k * tw_ref[...], first) * v
    yy = yy * lax.rsqrt(spread + GROUP_EPS) * hg_ref[...] + own
    mixed[tp] = (yy * jax.nn.sigmoid(gate_ref[...].astype(f32))).astype(bf16)
    mx = [
        rcopy(mixed.at[tp], mixed.at[tp], send.at[10], r_mx.at[d], t)
        for d, t in enumerate(others_tp)
    ]
    start(mx)
    serve(SERVE[3])
    wait_bytes(wo.at[0 : NX * LANES, :], r_wo.at[NX - 1])
    res_copy.wait()
    wait_recv(mx)

    wide = 256

    def project(n, ss):
        cut = pl.ds(pl.multiple_of(n * wide, wide), wide)
        lhs = jnp.concatenate([mixed[j] for j in range(NTP)], axis=1)
        mix = jnp.dot(lhs, wo[:, cut], preferred_element_type=f32)
        mix = mix.astype(bf16).astype(f32)
        a = (resid[:, cut].astype(f32) + mix).astype(bf16).astype(f32)
        after[:, cut] = a
        return ss + jnp.sum(a * a, axis=-1, keepdims=True)

    ss = lax.fori_loop(0, model // wide, project, jnp.zeros((steps, 1), f32))
    factor = lax.rsqrt(ss * (1.0 / model) + NORM_EPS)

    def scale(n, _):
        cut = pl.ds(pl.multiple_of(n * wide, wide), wide)
        normed[:, cut] = (after[:, cut] * factor * gain_ref[:, cut]).astype(bf16)
        return 0

    lax.fori_loop(0, model // wide, scale, 0)
    serve(len(work))
    wait_bytes(wall.at[0 : NZ * depth, 0:ca], r_yf.at[0])

    lo = 0
    while lo < ff:
        n = min(wide, ff - lo)
        g = jnp.dot(normed[...], wall[:, lo : lo + n], preferred_element_type=f32)
        u = jnp.dot(normed[...], wall[:, ff + lo : ff + lo + n], preferred_element_type=f32)
        hid[:, lo : lo + n] = (g / (1.0 + jnp.exp(-g)) * u).astype(bf16)
        lo += n

    def down_part(n, _):
        cut = pl.ds(pl.multiple_of(n * wide, wide), wide)
        d = lax.dot_general(hid[...], wall[cut, ca:], NT, preferred_element_type=f32)
        for t in range(NTP):
            parts[t % NC, t // NC, :, cut] = d[t * own_rows : (t + 1) * own_rows].astype(bf16)
        return 0

    lax.fori_loop(0, model // wide, down_part, 0)

    pair = rcopy(parts.at[1 - c], pair_in, send.at[11], r_pair.at[0], partner)
    pair.start()
    pair.wait_recv()
    pair_sum[...] = (parts[c].astype(f32) + pair_in[...].astype(f32)).astype(bf16)
    fin = []
    for d in range(1, NX):
        xx = (x + d) % NX
        cp = rcopy(pair_sum.at[xx], last_in.at[d - 1], send.at[12], r_last.at[d - 1], dev(tt=xx * NC + c))
        cp.start()
        fin.append(cp)
    total_down = parts[c, x].astype(f32) + pair_in[x].astype(f32)
    for d in range(1, NX):
        fin[d - 1].wait_recv()
        total_down = total_down + last_in[d - 1].astype(f32)
    mine = after[pl.ds(pl.multiple_of(tp * own_rows, 8), own_rows), :]
    out_ref[...] = (mine + total_down).astype(bf16)

    wait_bytes(wall.at[0 : (2 * HOPS - 1) * depth, 0:ca], send.at[0])
    wait_bytes(wall.at[0 : (2 * HOPS - 1) * plane, ca:], send.at[1])
    wait_bytes(wall.at[0 : 2 * NZ * depth, 0:ca], send.at[2])
    wait_bytes(wall.at[0 : NZ * depth, 0:ca], send.at[3])
    wait_bytes(wall.at[0 : (NY - 1) * depth, ca:], send.at[4])
    wait_bytes(wo.at[0 : (NX - 1) * LANES, :], send.at[5])
    wait_bytes(wo.at[0 : NX * LANES, :], send.at[6])
    wait_bytes(ybuf.at[0:3], send.at[7])
    wait_bytes(zbuf.at[0:3], send.at[8])
    for d in range(1, NG):
        @pl.when(zg + d < NG)
        def _(d=d):
            l3[d - 1].wait_send()
    wait_bytes(mixed.at[0 : NTP - 1], send.at[10])
    wait_bytes(pair_in, send.at[11])
    wait_bytes(pair_sum.at[0 : NX - 1], send.at[12])


SERVE = (3, 6, 6, 3)


def layer(r, k, v, dw, lw, gate, tw, hg, wg, wu, wd, gain, wo, residual):
    f32, bf16 = jnp.float32, jnp.bfloat16
    steps = r.shape[0]
    depth, ff = wg.shape
    model = residual.shape[1]
    own_rows = steps // NTP
    vmem = pl.BlockSpec(memory_space=pltpu.VMEM)
    far = pl.BlockSpec(memory_space=pl.ANY)
    dma = pltpu.SemaphoreType.DMA
    return pl.pallas_call(
        layer_kernel,
        in_specs=[vmem] * 12 + [far] * 2,
        out_specs=vmem,
        out_shape=jax.ShapeDtypeStruct((own_rows, model), bf16),
        scratch_shapes=[
            pltpu.VMEM((model, 3 * ff), bf16),
            pltpu.VMEM((NTP * LANES, model), bf16),
            pltpu.VMEM((NTP, steps, LANES), bf16),
            pltpu.VMEM((steps, model), bf16),
            pltpu.VMEM((steps, model), f32),
            pltpu.VMEM((steps, model), bf16),
            pltpu.VMEM((steps, ff), bf16),
            pltpu.VMEM((NC, NX, own_rows, model), bf16),
            pltpu.VMEM((NX, own_rows, model), bf16),
            pltpu.VMEM((NX, own_rows, model), bf16),
            pltpu.VMEM((NX - 1, own_rows, model), bf16),
            pltpu.VMEM((NY, PACKET, LANES), bf16),
            pltpu.VMEM((NG, PACKET, LANES), bf16),
            pltpu.VMEM((NG, PACKET, LANES), bf16),
            pltpu.VMEM((steps, LANES), f32),
            pltpu.VMEM((steps, LANES), f32),
            pltpu.VMEM((LANES, LANES), f32),
            dma((13,)),
            dma((NX,)),
            dma((2, HOPS)),
            dma((2, HOPS)),
            dma((2, NZ)),
            dma((1,)),
            dma((NY - 1,)),
            dma((NY - 1,)),
            dma((NG - 1,)),
            dma((NG - 1,)),
            dma((NTP - 1,)),
            dma((1,)),
            dma((NX - 1,)),
            dma((2,)),
        ],
        compiler_params=pltpu.CompilerParams(
            collective_id=0, has_side_effects=True, vmem_limit_bytes=60 * 1024 * 1024
        ),
        cost_estimate=pl.CostEstimate(
            flops=3_000_000_000, bytes_accessed=8_000_000, transcendentals=1_000_000
        ),
        name="layer",
    )(r, k, v, dw, lw, gate, tw, hg, wg, wu, wd, gain, wo, residual)


def per_device(r, k, v, dw, lw, gate, tw, hg, w_out, residual, gain, w_gate, w_up, w_down):
    return layer(
        r, k, v, dw, lw, gate, tw.reshape(1, -1), hg.reshape(1, -1), w_gate, w_up, w_down,
        gain.reshape(1, -1), w_out, residual,
    )


def solution(mesh):
    split_both = P("sp", "tp")
    placed = (split_both,) * 6 + (
        P("tp", None),
        P("tp"),
        P("tp", None),
        P("sp", None),
        P(),
        split_both,
        split_both,
        P("tp", "sp"),
    )
    return jax.shard_map(
        per_device, mesh=mesh, in_specs=placed, out_specs=P(("sp", "tp"), None), check_vma=False
    )
```

time: 393 us -> 101 us (0.26)
  blocking collectives: 167 us -> 0 us
  waiting for transfers between devices: 161 us -> 0 us
  Pallas kernels: 10.2 us -> 96.6 us
  starting transfers between devices: 23.9 us -> 0 us
  between operations: 13.5 us -> 0.01 us
  matrix products: 9.16 us -> 0 us
    all_gather x2 -> x0, waiting for transfers between devices: 142 us -> none  [the longest x1 142 us: per_device(): ps_all = lax.all_gather(ps, 'sp')]
    all_gather x4 -> x0, blocking collectives: 104 us -> none  [the longest x2 62.3 us: by_columns(): return lax.all_gather(w, 'sp', axis_index_groups=far, axis=0, tiled=False)]
    pallas_call x2 -> x1, Pallas kernels: 10.2 us -> 96.6 us  [layer(): pl.pallas_call(layer_kernel, in_specs=[vmem] * 12 + [far] * 2, out_specs=...]
    all_to_all x2 -> x0, blocking collectives: 63.6 us -> none  [the longest x1 38.4 us: per_device(): down = lax.all_to_all(down, 'tp', 0, 0)]
    all_to_all x4 -> x0, starting transfers between devices: 23.9 us -> none  [the longest x1 14.1 us: per_device(): mix = lax.all_to_all(part.reshape(tp, own_rows, -1), 'tp', 0, 0)]
    all_to_all x4 -> x0, waiting for transfers between devices: 19.4 us -> none  [the longest x1 12.2 us: per_device(): mix = lax.all_to_all(part.reshape(tp, own_rows, -1), 'tp', 0, 0)]
    dot_general x2 -> x0, matrix products: 9.16 us -> none  [the longest x1 6.07 us: per_device(): jnp.dot(h, d_all, preferred_element_type=jnp.float32).astype(jnp.bfloat16)]
  transfers between devices with their start and end apart: 6 -> 0, of which waited for: 4 -> 0; matrix products, arithmetic and copies ran while one was open for 1% -> 0% of each run, Pallas kernels for 0% -> 0%
where the time goes in v1:
time: 101 us
  Pallas kernels  96.6 us (96%)
  local copies, waits for them, and re-layouts  4.38 us (4%)
    pallas_call x1, Pallas kernels, layer(): pl.pallas_call(layer_kernel, in_specs=[vmem] * 12 + [far] * 2, out_specs=...  96.6 us
    unnamed x4, local copies, waits for them, and re-layouts  3.79 us

profile of v1, /device:TPU:1, one launch (start us, length us, event | category | flops | bytes accessed | tf_op | source)
XLA Modules:
  0.0 101.0 jit_solution(11688407404492887643)
XLA Ops:
  0.0 0.0 copy-start
  0.0 0.7 copy-done
  0.7 0.6 reshape.9.tw_ref
  1.3 1.6 %copy.15.wd_ref = bf16[640,32]{1,0:T(8,128)(2,1)} copy(bf16[640,32]{0,1:T(8,128)(2,1)} %param.27) | data formatting | bytes 81920 | tf_op args[13]
  2.8 96.6 %layer.1 = bf16[24,2048]{1,0:T(8,128)(2,1)} custom-call(bf16[192,128]{1,0:T(8,128)(2,1)} %r_ref.1, bf16[192,128]{1,0:T(8,128)(2,1)} %k_ref.1, bf16[192,128]{1,0:T(8,128)(2,1)} %v_ref.1, f32[192,128]{1,0:T(8,128)} %dw_ref.1, f32[192,128]{1,0:T(8,128)} %lw_ref.1, bf16[192,128]{1,0:T(8,128)(2,1)} %gate_ref.1, f32[1,128]{1,0:T(1,128)} %reshape.9.tw_ref, ...), custom_call_target="tpu_custom_call" | custom-call | flops 3000000000 | bytes 8000000 | tf_op jit(solution)/shard_map/layer/pallas_call | solution.py:521
  99.4 1.5 %copy.17 = bf16[24,2048]{1,0:T(8,128)(2,1)} copy(bf16[24,2048]{1,0:T(8,128)(2,1)} %layer.1) | data formatting | bytes 196608
Async XLA Ops:
  0.0 0.7 copy-start

commit v2 on v1

v2 whole, which is shorter than its diff:
```python
import functools

import jax
import jax.numpy as jnp
from jax import lax
from jax.experimental import pallas as pl
from jax.experimental.pallas import tpu as pltpu
from jax.sharding import PartitionSpec as P

HEAD = 64
LANES = 2 * HEAD
GROUP_EPS = 0.00064
NORM_EPS = 1e-06
NN = (((1,), (0,)), ((), ()))
NT = (((1,), (1,)), ((), ()))
TN = (((0,), (0,)), ((), ()))
NX, NY, NZ, NC = 4, 4, 16, 2
NTP = NX * NC
NG = 4
HOPS = NZ // 2
MESH = pl.DeviceIdType.MESH
PACKET = LANES + 16


def split(x):
    high = x.astype(jnp.bfloat16)
    return high, (x - high.astype(jnp.float32)).astype(jnp.bfloat16)


def dot1(a, b, dims=NN):
    return lax.dot_general(
        a.astype(jnp.bfloat16), b.astype(jnp.bfloat16), dims, preferred_element_type=jnp.float32
    )


def dot3(a, b, dims=NN):
    ah, al = a if isinstance(a, tuple) else split(a)
    bh, bl = b if isinstance(b, tuple) else split(b)
    d = functools.partial(
        lax.dot_general, dimension_numbers=dims, preferred_element_type=jnp.float32
    )
    return d(ah, bh) + (d(ah, bl) + d(al, bh))


def per_head_sum(x, first):
    s0 = jnp.sum(jnp.where(first, x, 0.0), axis=-1, keepdims=True)
    s1 = jnp.sum(jnp.where(first, 0.0, x), axis=-1, keepdims=True)
    return jnp.where(first, s0, s1)


def block_diag_mask():
    row = lax.broadcasted_iota(jnp.int32, (LANES, LANES), 0)
    col = lax.broadcasted_iota(jnp.int32, (LANES, LANES), 1)
    return row // HEAD == col // HEAD


def fold(full):
    kept = jnp.where(block_diag_mask(), full, 0.0)
    return kept[:HEAD] + kept[HEAD:]


def unfold(packed):
    return jnp.where(block_diag_mask(), jnp.concatenate([packed, packed], axis=0), 0.0)


def fold_diag(d):
    row = lax.broadcasted_iota(jnp.int32, (HEAD, LANES), 0)
    col = lax.broadcasted_iota(jnp.int32, (HEAD, LANES), 1)
    return jnp.where(col % HEAD == row, d, 0.0)


def compose(a, b):
    both = dot3(jnp.concatenate([a[0], a[1]], axis=0), unfold(b[0]))
    return both[:HEAD], both[HEAD:] + b[1]


def put_packet(ref, slot, prod, state, decay):
    high, low = split(decay)
    row = lax.broadcasted_iota(jnp.int32, (16, LANES), 0)
    high, low = high.astype(jnp.float32), low.astype(jnp.float32)
    tail = jnp.where(row == 0, high, jnp.where(row == 1, low, 0.0))
    ref[slot, :HEAD, :] = (prod - fold_diag(decay)).astype(jnp.bfloat16)
    ref[slot, HEAD:LANES, :] = state.astype(jnp.bfloat16)
    ref[slot, LANES:, :] = tail.astype(jnp.bfloat16)


def get_packet(ref, slot):
    f32 = jnp.float32
    tail = ref[slot, LANES:, :].astype(f32)
    decay = tail[0:1] + tail[1:2]
    prod = ref[slot, :HEAD, :].astype(f32) + fold_diag(decay)
    return prod, ref[slot, HEAD:LANES, :].astype(f32), decay


def local_part(r_ref, k_ref, v_ref, dw_ref, lw_ref, enter):
    steps = r_ref.shape[0]
    f32 = jnp.float32
    first = lax.broadcasted_iota(jnp.int32, (steps, LANES), 1) < HEAD
    row = lax.broadcasted_iota(jnp.int32, (steps, steps), 0)
    col = lax.broadcasted_iota(jnp.int32, (steps, steps), 1)
    r, k, v = (x[...].astype(f32) for x in (r_ref, k_ref, v_ref))
    log_decay = jax.nn.sigmoid(dw_ref[...]) * (-0.6065306597126334)
    ones = (row >= col).astype(jnp.bfloat16)
    h0 = log_decay.astype(jnp.bfloat16)
    rest = log_decay - h0.astype(f32)
    h1 = rest.astype(jnp.bfloat16)
    h2 = (rest - h1.astype(f32)).astype(jnp.bfloat16)
    total = dot1(ones, h0) + (dot1(ones, h1) + dot1(ones, h2))
    last = total[steps - 1 :, :]
    unit = k / jnp.maximum(jnp.sqrt(per_head_sum(k * k, first)), 1.0)
    insert = unit * jax.nn.sigmoid(lw_ref[...])
    undo = jnp.exp(-total)
    remaining = jnp.exp(last - total)
    a_bar = -unit * jnp.exp(total - log_decay)
    r_bar = r * jnp.exp(total)
    b_hat = insert * undo
    k_hat = k * undo
    right = split(jnp.concatenate([b_hat, k_hat], axis=0))
    left = jnp.concatenate([a_bar, r_bar], axis=0)
    first2 = jnp.concatenate([first, first], axis=0)
    grams = [
        dot3(jnp.where(first2 if h == 0 else ~first2, left, 0.0), right, NT) for h in (0, 1)
    ]
    enter()
    strict, incl = row > col, row >= col
    ab = [jnp.where(strict, g[:steps, :steps], 0.0) for g in grams]
    ak = [jnp.where(strict, g[:steps, steps:], 0.0) for g in grams]
    rb = [jnp.where(incl, g[steps:, :steps], 0.0) for g in grams]
    rk = [jnp.where(incl, g[steps:, steps:], 0.0) for g in grams]
    vb = v_ref[...]

    def times_v(m):
        mh, ml = split(m)
        return dot1(mh, vb) + dot1(ml, vb)

    seeds = [jnp.concatenate([a_bar, times_v(m)], axis=1) for m in ak]
    ab16 = [m.astype(jnp.bfloat16) for m in ab]
    eye = (row == col).astype(f32)
    size = 1
    inv = None
    while size < steps:
        joined = (
            (row // (2 * size) == col // (2 * size))
            & ((row // size) % 2 == 1)
            & ((col // size) % 2 == 0)
        )
        parts = [jnp.where(joined, m, jnp.zeros_like(m)) for m in ab16]
        if inv is None:
            inv = [eye + p.astype(f32) for p in parts]
        else:
            t16 = [t.astype(jnp.bfloat16) for t in inv]
            mid = [dot1(t, p) for t, p in zip(t16, parts)]
            inv = [t + dot1(m, tt) for t, m, tt in zip(inv, mid, t16)]
        size *= 2
    inv16 = [t.astype(jnp.bfloat16) for t in inv]
    absp = [split(m) for m in ab]
    sol = [dot1(t, s) for t, s in zip(inv16, seeds)]
    for _ in range(2):
        res = [s - x + dot3(m, x) for s, x, m in zip(seeds, sol, absp)]
        sol = [x + dot1(t, e) for x, t, e in zip(sol, inv16, res)]
    w = jnp.where(first, sol[0][:, :LANES], sol[1][:, :LANES])
    u = jnp.where(first, sol[0][:, LANES:], sol[1][:, LANES:])
    b_end = split(insert * remaining)
    decay = jnp.exp(last)
    prod = fold(dot3(w, b_end, TN)) + fold_diag(decay)
    kh, kl = split(k * remaining)
    state = fold(dot3(u, b_end, TN) + dot1(vb, kh, TN) + dot1(vb, kl, TN))

    def outputs():
        outs = [dot3(m, x) for m, x in zip(rb, sol)]
        own = [times_v(m) for m in rk]
        q = r_bar + jnp.where(first, outs[0][:, :LANES], outs[1][:, :LANES])
        y = jnp.where(first, outs[0][:, LANES:] + own[0], outs[1][:, LANES:] + own[1])
        return q, y

    return prod, state, decay, outputs


def layer_kernel(
    r_hbm, k_hbm, v_hbm, dw_hbm, lw_hbm, gate_hbm, tw_hbm, hg_hbm, gain_hbm, wg_hbm, wu_hbm, wd_hbm,
    wo_hbm, res_hbm,
    out_ref,
    wall, wo, mixed, resid, after, normed, hid, parts, pair_in, pair_sum, last_in,
    r_ref, k_ref, v_ref, dw_ref, lw_ref, gate_ref, tw_ref, hg_ref, gain_ref,
    ybuf, zbuf, gbuf, q_s, y_s, ent,
    send, r_wo, r_z, r_q, r_y0, r_ya, r_yb, r_l1, r_l2, r_l3, x_l3, r_l4, x_l4, r_mx, r_pair, r_last, loc,
):
    f32, bf16 = jnp.float32, jnp.bfloat16
    steps = r_ref.shape[0]
    depth, ff = wg_hbm.shape
    plane = NY * depth
    half = depth // 2
    ca = 2 * ff
    model = wo.shape[1]
    own_rows = out_ref.shape[0]
    sp, tp = lax.axis_index("sp"), lax.axis_index("tp")
    z, y = sp // NY, sp % NY
    x, c = tp // NC, tp % NC
    zg, zl = z // NG, z % NG

    def dev(zz=None, yy=None, tt=None):
        zz = z if zz is None else zz
        yy = y if yy is None else yy
        return (zz * NY + yy, tp if tt is None else tt)

    def rcopy(src, dst, s, r, device):
        return pltpu.make_async_remote_copy(
            src_ref=src, dst_ref=dst, send_sem=s, recv_sem=r, device_id=device, device_id_type=MESH
        )

    def wait_bytes(ref, sem):
        pltpu.make_async_copy(ref, ref, sem).wait()

    up, down = (z + 1) % NZ, (z + NZ - 1) % NZ
    others_y = [dev(yy=(y + d) % NY) for d in range(1, NY)]
    others_zl = [dev(zz=zg * NG + (zl + d) % NG) for d in range(1, NG)]
    others_zg = [dev(zz=((zg + d) % NG) * NG + zl) for d in range(1, NG)]
    others_tp = [dev(tt=(tp + d) % NTP) for d in range(1, NTP)]
    ring = [dev(zz=up), dev(zz=down)]

    barrier = pltpu.get_barrier_semaphore()
    greet = others_y + others_zl + others_zg + others_tp + ring
    for d in greet:
        pl.semaphore_signal(barrier, inc=1, device_id=d, device_id_type=MESH)

    my_row = pl.multiple_of(sp * depth, depth)
    wo_rows = lambda t: wo.at[pl.ds(pl.multiple_of(t * LANES, LANES), LANES), :]
    loads = [
        (dw_hbm, dw_ref), (k_hbm, k_ref), (lw_hbm, lw_ref), (r_hbm, r_ref), (v_hbm, v_ref),
        (wg_hbm, wall.at[pl.ds(my_row, depth), 0:ff]),
        (wu_hbm, wall.at[pl.ds(my_row, depth), ff:ca]),
        (wd_hbm, wall.at[pl.ds(my_row, depth), ca:]),
        (gate_hbm, gate_ref), (tw_hbm, tw_ref), (hg_hbm, hg_ref), (gain_hbm, gain_ref),
        (wo_hbm, wo_rows(tp)), (res_hbm, resid),
    ]
    loads = [pltpu.make_async_copy(a, b, loc.at[i]) for i, (a, b) in enumerate(loads)]
    for cp in loads:
        cp.start()

    def rows(zz, yy, lo=0, n=None):
        return pl.ds(pl.multiple_of(zz * plane + yy * depth + lo, half), depth if n is None else n)

    y2 = (y + 2) % NY
    lane = (y, y2)
    cols = (slice(0, ff), slice(ff, ca), slice(ca, 3 * ff))

    def block(zz, yy, part, lo=0, n=None):
        return wall.at[rows(zz, yy, lo, n), cols[part]]

    def ahead(s, dirn):
        return (z + NZ - s) % NZ if dirn == 0 else (z + s) % NZ

    def plane_of(i):
        return z if i == 0 else ahead((i + 1) // 2, (i - 1) % 2)

    def zstream(st, part, s):
        out = []
        for d in (0, 1):
            at = (0, depth) if s < HOPS - 1 else (half * d, half)
            ref = block(ahead(s, d), lane[st], part, *at)
            k = 3 * st + part
            out.append(rcopy(ref, ref, send.at[k], r_z.at[k, d, s], ring[d]))
        return out

    side = [dev(yy=(y + 1) % NY), dev(yy=(y + NY - 1) % NY)]

    def yside(part, i):
        ref = block(plane_of(i), y, part)
        sems = [r_ya.at[part]] * 2 if part < DOWN else [r_yb.at[d, i] for d in (0, 1)]
        if i == 0:
            sems = [r_y0.at[part, d] for d in (0, 1)]
        return [rcopy(ref, ref, send.at[6 + part], sems[d], side[d]) for d in (0, 1)]

    def across(part):
        out = []
        for d in (0, 1):
            ref = block(z, (y + NY - 1) % NY if d == 0 else (y + 1) % NY, part, half * d, half)
            out.append(rcopy(ref, ref, send.at[9 + part], r_q.at[part, d], side[d]))
        return out

    def start(copies):
        for cp in copies:
            cp.start()

    def wait_recv(copies):
        for cp in copies:
            cp.wait_recv()

    def exchange(buf, slot, sem, s, targets):
        return [
            rcopy(buf.at[slot], buf.at[slot], send.at[s], sem.at[d], t)
            for d, t in enumerate(targets)
        ]

    def wo_same(d):
        t = ((x + d) % NX) * NC + c
        return rcopy(wo_hbm, wo_rows(tp), send.at[12], r_wo.at[d - 1], dev(tt=t))

    partner = dev(tt=x * NC + 1 - c)

    def wo_relay(d):
        ref = wo_rows(((x + NX - d) % NX) * NC + c)
        return rcopy(ref, ref, send.at[13], r_wo.at[NX - 1], partner)

    def enter():
        for cp in loads[5:8]:
            cp.wait()
        with jax.named_scope("enter"):
            pl.semaphore_wait(barrier, len(greet))
        for part in range(3):
            start(zstream(0, part, 0))
            start(yside(part, 0))
        for d in range(1, NX):
            wo_same(d).start()

    def new_at(s):
        return [2 * s + 1, 2 * s + 2] if s < HOPS - 1 else [2 * s + 1]

    def relay(part):
        wait_recv(yside(part, 0))
        start(across(part))

    def q_open(part):
        wait_recv(across(part))
        start(zstream(1, part, 0))

    def p_step(part, s):
        wait_recv(zstream(0, part, s))
        if s < HOPS - 1:
            start(zstream(0, part, s + 1))
        for i in new_at(s):
            start(yside(part, i))

    def q_step(part, s):
        wait_recv(zstream(1, part, s))
        if s < HOPS - 1:
            start(zstream(1, part, s + 1))

    work = []

    def job(f, *a):
        work.append(functools.partial(f, *a))

    for part in range(DOWN):
        job(relay, part)
        job(p_step, part, 0)
    job(relay, DOWN)
    job(q_open, 0)
    job(q_open, 1)
    job(p_step, DOWN, 0)
    job(q_open, DOWN)
    for s in range(HOPS + LAG):
        for step in (p_step, q_step):
            for part in range(3):
                t = s - LAG if part == DOWN else s
                if 0 <= t < HOPS and (step is q_step or t > 0):
                    job(step, part, t)
    a_last = [f for f in work if f.args[0] < DOWN and f.func is q_step][-1]
    b_last = [f for f in work if f.args[0] == DOWN and f.func is q_step]

    def serve(n=None, until=None):
        while work and (n is None or n > 0) and (until is None or until in work):
            f = work.pop(0)
            n = None if n is None else n - 1
            with jax.named_scope("_".join([f.func.__name__] + [str(a) for a in f.args])):
                f()

    for cp in loads[:5]:
        cp.wait()
    with jax.named_scope("local"):
        prod, state, decay, outputs = local_part(r_ref, k_ref, v_ref, dw_ref, lw_ref, enter)
        put_packet(ybuf, y, prod, state, decay)
    l1 = exchange(ybuf, y, r_l1, 14, others_y)
    start(l1)
    with jax.named_scope("local_out"):
        q, y_own = outputs()
        q_s[...] = q
        y_s[...] = y_own
    for cp in loads[8:]:
        cp.wait()
    wo_relay(0).start()
    serve(SERVE[0])
    with jax.named_scope("wait_l1"):
        wait_recv(l1)

    def total(buf):
        m = [get_packet(buf, j) for j in range(4)]
        ab, cd = compose(m[0], m[1]), compose(m[2], m[3])
        return (*compose(ab, cd), (m[0][2] * m[1][2]) * (m[2][2] * m[3][2]))

    ident = (fold_diag(jnp.ones((1, LANES), f32)), jnp.zeros((HEAD, LANES), f32))

    def before(at, buf, count):
        ent[at] = jnp.concatenate(ident, axis=0)

        def step(j, _):
            p, u, _ = get_packet(buf, j)
            both = dot3(ent[at], unfold(p))
            ent[at, 0:HEAD, :] = both[:HEAD]
            ent[at, HEAD:, :] = both[HEAD:] + u
            return 0

        lax.fori_loop(0, count, step, 0)

    put_packet(zbuf, zl, *total(ybuf))
    l2 = exchange(zbuf, zl, r_l2, 15, others_zl)
    start(l2)
    with jax.named_scope("before_y"):
        before(0, ybuf, y)
    serve(SERVE[1])
    with jax.named_scope("wait_l2"):
        wait_recv(l2)
    put_packet(gbuf, zg, *total(zbuf))
    quarter = pl.ds(pl.multiple_of(y * (LANES // NY), LANES // NY), LANES // NY)

    def far(d):
        cuts = gbuf.at[zg, quarter, :], gbuf.at[zg, LANES:, :]
        return [
            rcopy(ref, ref, x_l3.at[d - 1, i], r_l3.at[d - 1, i], others_zg[d - 1])
            for i, ref in enumerate(cuts)
        ]

    def share(d):
        ref = gbuf.at[zg - d, quarter, :]
        return [
            rcopy(ref, ref, x_l4.at[d - 1, e], r_l4.at[d - 1, e], others_y[e])
            for e in range(NY - 1)
        ]

    for d in range(1, NG):
        @pl.when(zg + d < NG)
        def _(d=d):
            start(far(d))

    with jax.named_scope("before_z"):
        before(1, zbuf, zl)
    serve(SERVE[2])
    with jax.named_scope("wait_far"):
        for d in range(1, NG):
            @pl.when(zg >= d)
            def _(d=d):
                wait_recv(far(d))
                start(share(d))
    serve(SERVE[3])
    with jax.named_scope("relay"):
        for d in range(1, NX):
            wo_same(d).wait_recv()
            wo_relay(d).start()
    with jax.named_scope("wait_l3"):
        for d in range(1, NG):
            @pl.when(zg >= d)
            def _(d=d):
                wait_recv(share(d))

    def turn(j, s):
        p, u, _ = get_packet(gbuf, j)
        return dot3(s, unfold(p)) + u

    s_in = lax.fori_loop(0, zg, turn, jnp.zeros((HEAD, LANES), f32))
    for at in (1, 0):
        s_in = dot3(s_in, unfold(ent[at, 0:HEAD, :])) + ent[at, HEAD:, :]

    first = lax.broadcasted_iota(jnp.int32, (steps, LANES), 1) < HEAD
    yy = dot3(q_s[...], unfold(s_in), NT) + y_s[...]
    yy = yy - per_head_sum(yy, first) * (1.0 / HEAD)
    spread = per_head_sum(yy * yy, first) * (1.0 / HEAD)
    r, k, v = (a[...].astype(f32) for a in (r_ref, k_ref, v_ref))
    weight = jnp.concatenate([tw_ref[0:1, :], tw_ref[1:2, :]], axis=1)
    own = per_head_sum(r * k * weight, first) * v
    yy = yy * lax.rsqrt(spread + GROUP_EPS) * hg_ref[...] + own
    mixed[tp] = (yy * jax.nn.sigmoid(gate_ref[...].astype(f32))).astype(bf16)
    mx = [
        rcopy(mixed.at[tp], mixed.at[tp], send.at[17], r_mx.at[d], t)
        for d, t in enumerate(others_tp)
    ]
    start(mx)
    serve(SERVE[4])
    with jax.named_scope("wait_mixed"):
        wait_bytes(wo.at[0 : NX * LANES, :], r_wo.at[NX - 1])
        wait_recv(mx)

    wide = 512

    def project(n, ss):
        cut = pl.ds(pl.multiple_of(n * wide, wide), wide)
        lhs = jnp.concatenate([mixed[j] for j in range(NTP)], axis=1)
        mix = jnp.dot(lhs, wo[:, cut], preferred_element_type=f32)
        mix = mix.astype(bf16).astype(f32)
        a = (resid[:, cut].astype(f32) + mix).astype(bf16).astype(f32)
        after[:, cut] = a
        return ss + jnp.sum(a * a, axis=-1, keepdims=True)

    with jax.named_scope("project"):
        ss = lax.fori_loop(0, model // wide, project, jnp.zeros((steps, 1), f32))
    factor = lax.rsqrt(ss * (1.0 / model) + NORM_EPS)

    def scale(n, _):
        cut = pl.ds(pl.multiple_of(n * wide, wide), wide)
        normed[:, cut] = (after[:, cut] * factor * gain_ref[:, cut]).astype(bf16)
        return 0

    with jax.named_scope("scale"):
        lax.fori_loop(0, model // wide, scale, 0)
    serve(until=a_last)
    serve(1)
    with jax.named_scope("wait_gate_up"):
        for part in range(DOWN):
            wait_bytes(wall.at[0 : 2 * (NZ - 1) * depth, cols[part]], r_ya.at[part])

    serve(1)
    with jax.named_scope("gate_up"):
        lo = 0
        while lo < ff:
            n = min(256, ff - lo)
            g = jnp.dot(normed[...], wall[:, lo : lo + n], preferred_element_type=f32)
            u = jnp.dot(normed[...], wall[:, ff + lo : ff + lo + n], preferred_element_type=f32)
            hid[:, lo : lo + n] = (g / (1.0 + jnp.exp(-g)) * u).astype(bf16)
            lo += n

    serve(1)

    def down_planes(lo, hi):
        for i in range(lo, hi, 2):
            both = [wall[rows(plane_of(j), 0, 0, plane), ca:] for j in range(i, min(i + 2, hi))]
            w = both[0] if len(both) == 1 else jnp.concatenate(both, axis=0)
            d = lax.dot_general(hid[...], w, NT, preferred_element_type=f32)
            for t in range(NTP):
                own = d[t * own_rows : (t + 1) * own_rows].astype(bf16)
                for j in range(len(both)):
                    parts[t % NC, i + j, t // NC] = own[:, j * plane : (j + 1) * plane]

    def pair(g):
        lo, hi = GROUPS[g]
        return rcopy(
            parts.at[1 - c, lo:hi], pair_in.at[lo:hi], send.at[18], r_pair.at[g], partner
        )

    def across_x(g):
        lo, hi = GROUPS[g]
        out = []
        for d in range(1, NX):
            xx = (x + d) % NX
            out.append(
                rcopy(
                    pair_sum.at[xx, lo:hi], last_in.at[d - 1, lo:hi], send.at[19],
                    r_last.at[d - 1, g], dev(tt=xx * NC + c),
                )
            )
        return out

    def sum_pair(g):
        with jax.named_scope(f"pair_{g}"):
            pair(g).wait_recv()
        lo, hi = GROUPS[g]
        for xx in range(NX):
            both = parts[c, lo:hi, xx].astype(f32) + pair_in[lo:hi, xx].astype(f32)
            pair_sum[xx, lo:hi] = both.astype(bf16)
        start(across_x(g))

    for g, (lo, hi) in enumerate(GROUPS):
        if g == 2 or b_last[hi // 2 - 1] in work:
            serve()
        with jax.named_scope(f"wait_down_{g}"):
            for i in range(max(lo, 1), hi):
                wait_recv(yside(DOWN, i))
        with jax.named_scope(f"down_{g}"):
            down_planes(lo, hi)
        pair(g).start()
        if g > 0:
            sum_pair(g - 1)
    sum_pair(len(GROUPS) - 1)

    my_rows = pl.ds(pl.multiple_of(tp * own_rows, 8), own_rows)
    for g, (lo, hi) in enumerate(GROUPS):
        with jax.named_scope(f"last_{g}"):
            wait_recv(across_x(g))
        for i in range(lo, hi):
            to = pl.ds(pl.multiple_of(plane_of(i) * plane, plane), plane)
            t = parts[c, i, x].astype(f32) + pair_in[i, x].astype(f32)
            for d in range(1, NX):
                t = t + last_in[d - 1, i].astype(f32)
            out_ref[:, to] = after[my_rows, to] + t

    for k in range(6):
        wait_bytes(wall.at[0 : (2 * HOPS - 1) * depth, cols[k % 3]], send.at[k])
    for part in range(3):
        wait_bytes(wall.at[0 : 2 * NZ * depth, cols[part]], send.at[6 + part])
        wait_bytes(wall.at[0:depth, cols[part]], send.at[9 + part])
    wait_bytes(wo.at[0 : (NX - 1) * LANES, :], send.at[12])
    wait_bytes(wo.at[0 : NX * LANES, :], send.at[13])
    wait_bytes(ybuf.at[0:3], send.at[14])
    wait_bytes(zbuf.at[0:3], send.at[15])
    for d in range(1, NG):
        @pl.when(zg + d < NG)
        def _(d=d):
            for cp in far(d):
                cp.wait_send()
    for d in range(1, NG):
        @pl.when(zg >= d)
        def _(d=d):
            for cp in share(d):
                cp.wait_send()
    wait_bytes(mixed.at[0 : NTP - 1], send.at[17])
    wait_bytes(pair_in, send.at[18])
    wait_bytes(pair_sum.at[0 : NX - 1], send.at[19])


DOWN = 2
LAG = 2
GROUPS = ((0, 5), (5, 9), (9, 13), (13, 15), (15, 16))
VMEM_MB = 58
SERVE = (4, 5, 11, 6, 9)


def layer(r, k, v, dw, lw, gate, tw, hg, wg, wu, wd, gain, wo, residual):
    f32, bf16 = jnp.float32, jnp.bfloat16
    steps = r.shape[0]
    depth, ff = wg.shape
    model = residual.shape[1]
    own_rows = steps // NTP
    vmem = pl.BlockSpec(memory_space=pltpu.VMEM)
    dma = pltpu.SemaphoreType.DMA
    return pl.pallas_call(
        layer_kernel,
        in_specs=[pl.BlockSpec(memory_space=pltpu.HBM)] * 14,
        out_specs=vmem,
        out_shape=pltpu.VMEM((own_rows, model), f32),
        scratch_shapes=[
            pltpu.VMEM((model, 3 * ff), bf16),
            pltpu.VMEM((NTP * LANES, model), bf16),
            pltpu.VMEM((NTP, steps, LANES), bf16),
            pltpu.VMEM((steps, model), bf16),
            pltpu.VMEM((steps, model), f32),
            pltpu.VMEM((steps, model), bf16),
            pltpu.VMEM((steps, ff), bf16),
            pltpu.VMEM((NC, NZ, NX, own_rows, LANES), bf16),
            pltpu.VMEM((NZ, NX, own_rows, LANES), bf16),
            pltpu.VMEM((NX, NZ, own_rows, LANES), bf16),
            pltpu.VMEM((NX - 1, NZ, own_rows, LANES), bf16),
            *[pltpu.VMEM(a.shape, a.dtype) for a in (r, k, v, dw, lw, gate, tw, hg, gain)],
            pltpu.VMEM((NY, PACKET, LANES), bf16),
            pltpu.VMEM((NG, PACKET, LANES), bf16),
            pltpu.VMEM((NG, PACKET, LANES), bf16),
            pltpu.VMEM((steps, LANES), f32),
            pltpu.VMEM((steps, LANES), f32),
            pltpu.VMEM((2, LANES, LANES), f32),
            dma((20,)),
            dma((NX,)),
            dma((6, 2, HOPS)),
            dma((3, 2)),
            dma((3, 2)),
            dma((DOWN,)),
            dma((2, NZ)),
            dma((NY - 1,)),
            dma((NG - 1,)),
            dma((NG - 1, 2)),
            dma((NG - 1, 2)),
            dma((NG - 1, NY - 1)),
            dma((NG - 1, NY - 1)),
            dma((NTP - 1,)),
            dma((len(GROUPS),)),
            dma((NX - 1, len(GROUPS))),
            dma((14,)),
        ],
        compiler_params=pltpu.CompilerParams(
            collective_id=0, has_side_effects=True, vmem_limit_bytes=VMEM_MB * 1024 * 1024
        ),
        cost_estimate=pl.CostEstimate(
            flops=3_000_000_000, bytes_accessed=8_000_000, transcendentals=1_000_000
        ),
        name="layer",
    )(r, k, v, dw, lw, gate, tw, hg, gain, wg, wu, wd, wo, residual)


def per_device(r, k, v, dw, lw, gate, tw, hg, w_out, residual, gain, w_gate, w_up, w_down):
    return layer(
        r, k, v, dw, lw, gate, tw, hg.reshape(1, -1), w_gate, w_up, w_down.T,
        gain.reshape(1, -1), w_out, residual,
    ).astype(jnp.bfloat16)


def solution(mesh):
    split_both = P("sp", "tp")
    placed = (split_both,) * 6 + (
        P("tp", None),
        P("tp"),
        P("tp", None),
        P("sp", None),
        P(),
        split_both,
        split_both,
        P("tp", "sp"),
    )
    return jax.shard_map(
        per_device, mesh=mesh, in_specs=placed, out_specs=P(("sp", "tp"), None), check_vma=False
    )
```

time: 101 us -> 83.5 us (0.83)
  Pallas kernels: 96.6 us -> 82.7 us
  local copies, waits for them, and re-layouts: 4.38 us -> 0 us
    pallas_call x1, Pallas kernels: 96.6 us -> 82.7 us  [layer(): pl.pallas_call(layer_kernel, in_specs=[pl.BlockSpec(memory_space=pltpu.HB...]
    unnamed x4 -> x0, local copies, waits for them, and re-layouts: 3.79 us -> none
where the time goes in v2:
time: 83.5 us; the launch traced here: 83.3 us
  Pallas kernels  82.7 us (99%)
    pallas_call x1, Pallas kernels, layer(): pl.pallas_call(layer_kernel, in_specs=[pl.BlockSpec(memory_space=pltpu.HB...  82.7 us

profile of v2, /device:TPU:1, one launch (start us, length us, event | category | flops | bytes accessed | tf_op | source)
XLA Modules:
  0.0 83.3 jit_solution(13938186700228440471)
XLA Ops:
  0.0 82.7 %layer.1 = f32[24,2048]{1,0:T(8,128)S(1)} custom-call(bf16[192,128]{1,0:T(8,128)(2,1)} %r_hbm.1, bf16[192,128]{1,0:T(8,128)(2,1)} %k_hbm.1, bf16[192,128]{1,0:T(8,128)(2,1)} %v_hbm.1, f32[192,128]{1,0:T(8,128)} %dw_hbm.1, f32[192,128]{1,0:T(8,128)} %lw_hbm.1, bf16[192,128]{1,0:T(8,128)(2,1)} %gate_hbm.1, f32[2,64]{1,0:T(2,128)} %tw_hbm.1, f32[1,128]{1,0:T(1,128)} %bitcast.5, ...), custom_call_target="tpu_custom_call" | custom-call | flops 3000000000 | bytes 8000000 | tf_op jit(solution)/shard_map/layer/pallas_call | solution.py:623
  82.7 0.7 convert_element_type.3

commit v3 on v2

--- a/solution.py
+++ b/solution.py
@@ -92,7 +92,7 @@
     return prod, ref[slot, HEAD:LANES, :].astype(f32), decay
 
 
-def local_part(r_ref, k_ref, v_ref, dw_ref, lw_ref, enter):
+def local_part(r_ref, k_ref, v_ref, dw_ref, lw_ref, between):
     steps = r_ref.shape[0]
     f32 = jnp.float32
     first = lax.broadcasted_iota(jnp.int32, (steps, LANES), 1) < HEAD
@@ -121,7 +121,7 @@
     grams = [
         dot3(jnp.where(first2 if h == 0 else ~first2, left, 0.0), right, NT) for h in (0, 1)
     ]
-    enter()
+    between()
     strict, incl = row > col, row >= col
     ab = [jnp.where(strict, g[:steps, :steps], 0.0) for g in grams]
     ak = [jnp.where(strict, g[:steps, steps:], 0.0) for g in grams]
@@ -226,15 +226,15 @@
     my_row = pl.multiple_of(sp * depth, depth)
     wo_rows = lambda t: wo.at[pl.ds(pl.multiple_of(t * LANES, LANES), LANES), :]
     loads = [
-        (dw_hbm, dw_ref), (k_hbm, k_ref), (lw_hbm, lw_ref), (r_hbm, r_ref), (v_hbm, v_ref),
         (wg_hbm, wall.at[pl.ds(my_row, depth), 0:ff]),
         (wu_hbm, wall.at[pl.ds(my_row, depth), ff:ca]),
         (wd_hbm, wall.at[pl.ds(my_row, depth), ca:]),
+        (dw_hbm, dw_ref), (k_hbm, k_ref), (lw_hbm, lw_ref), (r_hbm, r_ref), (v_hbm, v_ref),
         (gate_hbm, gate_ref), (tw_hbm, tw_ref), (hg_hbm, hg_ref), (gain_hbm, gain_ref),
         (wo_hbm, wo_rows(tp)), (res_hbm, resid),
     ]
     loads = [pltpu.make_async_copy(a, b, loc.at[i]) for i, (a, b) in enumerate(loads)]
-    for cp in loads:
+    for cp in loads[:8]:
         cp.start()
 
     def rows(zz, yy, lo=0, n=None):
@@ -259,23 +259,24 @@
             at = (0, depth) if s < HOPS - 1 else (half * d, half)
             ref = block(ahead(s, d), lane[st], part, *at)
             k = 3 * st + part
-            out.append(rcopy(ref, ref, send.at[k], r_z.at[k, d, s], ring[d]))
+            out.append(rcopy(ref, ref, send.at[k], r_z.at[k, s], ring[d]))
         return out
 
     side = [dev(yy=(y + 1) % NY), dev(yy=(y + NY - 1) % NY)]
 
     def yside(part, i):
         ref = block(plane_of(i), y, part)
-        sems = [r_ya.at[part]] * 2 if part < DOWN else [r_yb.at[d, i] for d in (0, 1)]
+        group = [g for g, (lo, hi) in enumerate(GROUPS) if lo <= i < hi][0]
+        sems = [r_ya.at[part] if part < DOWN else r_yb.at[group]] * 2
         if i == 0:
-            sems = [r_y0.at[part, d] for d in (0, 1)]
+            sems = [r_y0.at[part]] * 2
         return [rcopy(ref, ref, send.at[6 + part], sems[d], side[d]) for d in (0, 1)]
 
     def across(part):
         out = []
         for d in (0, 1):
             ref = block(z, (y + NY - 1) % NY if d == 0 else (y + 1) % NY, part, half * d, half)
-            out.append(rcopy(ref, ref, send.at[9 + part], r_q.at[part, d], side[d]))
+            out.append(rcopy(ref, ref, send.at[9 + part], r_q.at[part], side[d]))
         return out
 
     def start(copies):
@@ -288,7 +289,7 @@
 
     def exchange(buf, slot, sem, s, targets):
         return [
-            rcopy(buf.at[slot], buf.at[slot], send.at[s], sem.at[d], t)
+            rcopy(buf.at[slot], buf.at[slot], send.at[s], sem.at[0], t)
             for d, t in enumerate(targets)
         ]
 
@@ -303,13 +304,15 @@
         return rcopy(ref, ref, send.at[13], r_wo.at[NX - 1], partner)
 
     def enter():
-        for cp in loads[5:8]:
+        for cp in loads[:3]:
             cp.wait()
         with jax.named_scope("enter"):
             pl.semaphore_wait(barrier, len(greet))
         for part in range(3):
             start(zstream(0, part, 0))
             start(yside(part, 0))
+        for cp in loads[8:]:
+            cp.start()
         for d in range(1, NX):
             wo_same(d).start()
 
@@ -317,22 +320,25 @@
         return [2 * s + 1, 2 * s + 2] if s < HOPS - 1 else [2 * s + 1]
 
     def relay(part):
-        wait_recv(yside(part, 0))
+        wait_blocks(part, 2, r_y0.at[part])
         start(across(part))
 
+    def wait_blocks(part, n, sem):
+        wait_bytes(wall.at[0 : n * depth, cols[part]], sem)
+
     def q_open(part):
-        wait_recv(across(part))
+        wait_blocks(part, 1, r_q.at[part])
         start(zstream(1, part, 0))
 
     def p_step(part, s):
-        wait_recv(zstream(0, part, s))
+        wait_blocks(part, 2 if s < HOPS - 1 else 1, r_z.at[part, s])
         if s < HOPS - 1:
             start(zstream(0, part, s + 1))
         for i in new_at(s):
             start(yside(part, i))
 
     def q_step(part, s):
-        wait_recv(zstream(1, part, s))
+        wait_blocks(part, 2 if s < HOPS - 1 else 1, r_z.at[3 + part, s])
         if s < HOPS - 1:
             start(zstream(1, part, s + 1))
 
@@ -341,20 +347,20 @@
     def job(f, *a):
         work.append(functools.partial(f, *a))
 
-    for part in range(DOWN):
+    for part in range(3):
         job(relay, part)
+    for part in range(3):
         job(p_step, part, 0)
-    job(relay, DOWN)
     job(q_open, 0)
-    job(q_open, 1)
-    job(p_step, DOWN, 0)
-    job(q_open, DOWN)
-    for s in range(HOPS + LAG):
-        for step in (p_step, q_step):
+    for s in range(1, HOPS + LAG + 1):
+        for step, t in ((p_step, s), (q_step, s - 1)):
             for part in range(3):
-                t = s - LAG if part == DOWN else s
-                if 0 <= t < HOPS and (step is q_step or t > 0):
-                    job(step, part, t)
+                u = t - LAG if part == DOWN else t
+                if (0 if step is q_step else 1) <= u < HOPS:
+                    job(step, part, u)
+                if s == 1 and step is p_step and part == 0:
+                    job(q_open, 1)
+                    job(q_open, DOWN)
     a_last = [f for f in work if f.args[0] < DOWN and f.func is q_step][-1]
     b_last = [f for f in work if f.args[0] == DOWN and f.func is q_step]
 
@@ -365,13 +371,16 @@
             with jax.named_scope("_".join([f.func.__name__] + [str(a) for a in f.args])):
                 f()
 
-    for cp in loads[:5]:
+    for cp in loads[3:8]:
         cp.wait()
     with jax.named_scope("local"):
-        prod, state, decay, outputs = local_part(r_ref, k_ref, v_ref, dw_ref, lw_ref, enter)
+        prod, state, decay, outputs = local_part(
+            r_ref, k_ref, v_ref, dw_ref, lw_ref, enter
+        )
         put_packet(ybuf, y, prod, state, decay)
     l1 = exchange(ybuf, y, r_l1, 14, others_y)
     start(l1)
+    serve(SERVE[0])
     with jax.named_scope("local_out"):
         q, y_own = outputs()
         q_s[...] = q
@@ -379,9 +388,9 @@
     for cp in loads[8:]:
         cp.wait()
     wo_relay(0).start()
-    serve(SERVE[0])
+    serve(SERVE[1])
     with jax.named_scope("wait_l1"):
-        wait_recv(l1)
+        wait_bytes(ybuf.at[0:3], r_l1.at[0])
 
     def total(buf):
         m = [get_packet(buf, j) for j in range(4)]
@@ -407,23 +416,22 @@
     start(l2)
     with jax.named_scope("before_y"):
         before(0, ybuf, y)
-    serve(SERVE[1])
+    serve(SERVE[2])
     with jax.named_scope("wait_l2"):
-        wait_recv(l2)
+        wait_bytes(zbuf.at[0:3], r_l2.at[0])
     put_packet(gbuf, zg, *total(zbuf))
     quarter = pl.ds(pl.multiple_of(y * (LANES // NY), LANES // NY), LANES // NY)
 
     def far(d):
         cuts = gbuf.at[zg, quarter, :], gbuf.at[zg, LANES:, :]
         return [
-            rcopy(ref, ref, x_l3.at[d - 1, i], r_l3.at[d - 1, i], others_zg[d - 1])
-            for i, ref in enumerate(cuts)
+            rcopy(ref, ref, x_l3.at[d - 1], r_l3.at[d - 1], others_zg[d - 1]) for ref in cuts
         ]
 
     def share(d):
         ref = gbuf.at[zg - d, quarter, :]
         return [
-            rcopy(ref, ref, x_l4.at[d - 1, e], r_l4.at[d - 1, e], others_y[e])
+            rcopy(ref, ref, x_l4.at[d - 1], r_l4.at[d - 1], others_y[e])
             for e in range(NY - 1)
         ]
 
@@ -434,14 +442,14 @@
 
     with jax.named_scope("before_z"):
         before(1, zbuf, zl)
-    serve(SERVE[2])
+    serve(SERVE[3])
     with jax.named_scope("wait_far"):
         for d in range(1, NG):
             @pl.when(zg >= d)
             def _(d=d):
-                wait_recv(far(d))
+                wait_bytes(gbuf.at[0, 0 : LANES // NY + 16, :], r_l3.at[d - 1])
                 start(share(d))
-    serve(SERVE[3])
+    serve(SERVE[4])
     with jax.named_scope("relay"):
         for d in range(1, NX):
             wo_same(d).wait_recv()
@@ -450,7 +458,7 @@
         for d in range(1, NG):
             @pl.when(zg >= d)
             def _(d=d):
-                wait_recv(share(d))
+                wait_bytes(gbuf.at[0, 0 : LANES // NY * (NY - 1), :], r_l4.at[d - 1])
 
     def turn(j, s):
         p, u, _ = get_packet(gbuf, j)
@@ -470,14 +478,14 @@
     yy = yy * lax.rsqrt(spread + GROUP_EPS) * hg_ref[...] + own
     mixed[tp] = (yy * jax.nn.sigmoid(gate_ref[...].astype(f32))).astype(bf16)
     mx = [
-        rcopy(mixed.at[tp], mixed.at[tp], send.at[17], r_mx.at[d], t)
+        rcopy(mixed.at[tp], mixed.at[tp], send.at[17], r_mx.at[0], t)
         for d, t in enumerate(others_tp)
     ]
     start(mx)
-    serve(SERVE[4])
+    serve(SERVE[5])
     with jax.named_scope("wait_mixed"):
         wait_bytes(wo.at[0 : NX * LANES, :], r_wo.at[NX - 1])
-        wait_recv(mx)
+        wait_bytes(mixed.at[0 : NTP - 1], r_mx.at[0])
 
     wide = 512
 
@@ -502,12 +510,11 @@
     with jax.named_scope("scale"):
         lax.fori_loop(0, model // wide, scale, 0)
     serve(until=a_last)
-    serve(1)
+    serve(TAIL[0])
     with jax.named_scope("wait_gate_up"):
         for part in range(DOWN):
             wait_bytes(wall.at[0 : 2 * (NZ - 1) * depth, cols[part]], r_ya.at[part])
 
-    serve(1)
     with jax.named_scope("gate_up"):
         lo = 0
         while lo < ff:
@@ -517,7 +524,7 @@
             hid[:, lo : lo + n] = (g / (1.0 + jnp.exp(-g)) * u).astype(bf16)
             lo += n
 
-    serve(1)
+    serve(TAIL[1])
 
     def down_planes(lo, hi):
         for i in range(lo, hi, 2):
@@ -543,7 +550,7 @@
             out.append(
                 rcopy(
                     pair_sum.at[xx, lo:hi], last_in.at[d - 1, lo:hi], send.at[19],
-                    r_last.at[d - 1, g], dev(tt=xx * NC + c),
+                    r_last.at[g], dev(tt=xx * NC + c),
                 )
             )
         return out
@@ -558,11 +565,10 @@
         start(across_x(g))
 
     for g, (lo, hi) in enumerate(GROUPS):
-        if g == 2 or b_last[hi // 2 - 1] in work:
-            serve()
+        if b_last[hi // 2 - 1] in work:
+            serve(until=b_last[hi // 2 - 1])
         with jax.named_scope(f"wait_down_{g}"):
-            for i in range(max(lo, 1), hi):
-                wait_recv(yside(DOWN, i))
+            wait_blocks(DOWN, 2 * (hi - max(lo, 1)), r_yb.at[g])
         with jax.named_scope(f"down_{g}"):
             down_planes(lo, hi)
         pair(g).start()
@@ -573,7 +579,7 @@
     my_rows = pl.ds(pl.multiple_of(tp * own_rows, 8), own_rows)
     for g, (lo, hi) in enumerate(GROUPS):
         with jax.named_scope(f"last_{g}"):
-            wait_recv(across_x(g))
+            wait_bytes(last_in.at[:, lo:hi], r_last.at[g])
         for i in range(lo, hi):
             to = pl.ds(pl.multiple_of(plane_of(i) * plane, plane), plane)
             t = parts[c, i, x].astype(f32) + pair_in[i, x].astype(f32)
@@ -581,6 +587,8 @@
                 t = t + last_in[d - 1, i].astype(f32)
             out_ref[:, to] = after[my_rows, to] + t
 
+    drain = jax.named_scope("drain")
+    drain.__enter__()
     for k in range(6):
         wait_bytes(wall.at[0 : (2 * HOPS - 1) * depth, cols[k % 3]], send.at[k])
     for part in range(3):
@@ -593,23 +601,23 @@
     for d in range(1, NG):
         @pl.when(zg + d < NG)
         def _(d=d):
-            for cp in far(d):
-                cp.wait_send()
+            wait_bytes(gbuf.at[0, 0 : LANES // NY + 16, :], x_l3.at[d - 1])
     for d in range(1, NG):
         @pl.when(zg >= d)
         def _(d=d):
-            for cp in share(d):
-                cp.wait_send()
+            wait_bytes(gbuf.at[0, 0 : LANES // NY * (NY - 1), :], x_l4.at[d - 1])
     wait_bytes(mixed.at[0 : NTP - 1], send.at[17])
     wait_bytes(pair_in, send.at[18])
     wait_bytes(pair_sum.at[0 : NX - 1], send.at[19])
+    drain.__exit__(None, None, None)
 
 
 DOWN = 2
-LAG = 2
+LAG = 1
 GROUPS = ((0, 5), (5, 9), (9, 13), (13, 15), (15, 16))
 VMEM_MB = 58
-SERVE = (4, 5, 11, 6, 9)
+SERVE = (6, 1, 6, 9, 6, 9)
+TAIL = (0, 1)
 
 
 def layer(r, k, v, dw, lw, gate, tw, hg, wg, wu, wd, gain, wo, residual):
@@ -646,20 +654,20 @@
             pltpu.VMEM((2, LANES, LANES), f32),
             dma((20,)),
             dma((NX,)),
-            dma((6, 2, HOPS)),
-            dma((3, 2)),
-            dma((3, 2)),
+            dma((6, HOPS)),
+            dma((3,)),
+            dma((3,)),
             dma((DOWN,)),
-            dma((2, NZ)),
-            dma((NY - 1,)),
+            dma((len(GROUPS),)),
+            dma((1,)),
+            dma((1,)),
             dma((NG - 1,)),
-            dma((NG - 1, 2)),
-            dma((NG - 1, 2)),
-            dma((NG - 1, NY - 1)),
-            dma((NG - 1, NY - 1)),
-            dma((NTP - 1,)),
+            dma((NG - 1,)),
+            dma((NG - 1,)),
+            dma((NG - 1,)),
+            dma((1,)),
             dma((len(GROUPS),)),
-            dma((NX - 1, len(GROUPS))),
+            dma((len(GROUPS),)),
             dma((14,)),
         ],
         compiler_params=pltpu.CompilerParams(

time: 83.5 us -> 77.8 us (0.932)
  Pallas kernels: 82.7 us -> 77 us
    pallas_call x1, Pallas kernels: 82.7 us -> 77 us  [layer(): pl.pallas_call(layer_kernel, in_specs=[pl.BlockSpec(memory_space=pltpu.HB...]
where the time goes in v3:
time: 77.8 us; the launch traced here: 77.7 us
  Pallas kernels  77 us (99%)
    pallas_call x1, Pallas kernels, layer(): pl.pallas_call(layer_kernel, in_specs=[pl.BlockSpec(memory_space=pltpu.HB...  77 us

profile of v3, /device:TPU:1, one launch (start us, length us, event | category | flops | bytes accessed | tf_op | source)
XLA Modules:
  0.0 77.7 jit_solution(8404252713514074630)
XLA Ops:
  0.0 77.0 %layer.1 = f32[24,2048]{1,0:T(8,128)S(1)} custom-call(bf16[192,128]{1,0:T(8,128)(2,1)} %r_hbm.1, bf16[192,128]{1,0:T(8,128)(2,1)} %k_hbm.1, bf16[192,128]{1,0:T(8,128)(2,1)} %v_hbm.1, f32[192,128]{1,0:T(8,128)} %dw_hbm.1, f32[192,128]{1,0:T(8,128)} %lw_hbm.1, bf16[192,128]{1,0:T(8,128)(2,1)} %gate_hbm.1, f32[2,64]{1,0:T(2,128)} %tw_hbm.1, f32[1,128]{1,0:T(1,128)} %bitcast.5, ...), custom_call_target="tpu_custom_call" | custom-call | flops 3000000000 | bytes 8000000 | tf_op jit(solution)/shard_map/layer/pallas_call | solution.py:631
  77.0 0.7 convert_element_type.3

commit v4 on v3

--- a/solution.py
+++ b/solution.py
@@ -121,7 +121,6 @@
     grams = [
         dot3(jnp.where(first2 if h == 0 else ~first2, left, 0.0), right, NT) for h in (0, 1)
     ]
-    between()
     strict, incl = row > col, row >= col
     ab = [jnp.where(strict, g[:steps, :steps], 0.0) for g in grams]
     ak = [jnp.where(strict, g[:steps, steps:], 0.0) for g in grams]
@@ -152,6 +151,7 @@
             mid = [dot1(t, p) for t, p in zip(t16, parts)]
             inv = [t + dot1(m, tt) for t, m, tt in zip(inv, mid, t16)]
         size *= 2
+    between()
     inv16 = [t.astype(jnp.bfloat16) for t in inv]
     absp = [split(m) for m in ab]
     sol = [dot1(t, s) for t, s in zip(inv16, seeds)]
@@ -183,7 +183,7 @@
     wall, wo, mixed, resid, after, normed, hid, parts, pair_in, pair_sum, last_in,
     r_ref, k_ref, v_ref, dw_ref, lw_ref, gate_ref, tw_ref, hg_ref, gain_ref,
     ybuf, zbuf, gbuf, q_s, y_s, ent,
-    send, r_wo, r_z, r_q, r_y0, r_ya, r_yb, r_l1, r_l2, r_l3, x_l3, r_l4, x_l4, r_mx, r_pair, r_last, loc,
+    send, r_wo, r_z, r_q, r_y0, r_ya, r_yb, r_l1, r_l2, r_l3, x_l3, r_l4, x_l4, r_mx, r_pair, r_last, loc, ok,
 ):
     f32, bf16 = jnp.float32, jnp.bfloat16
     steps = r_ref.shape[0]
@@ -219,7 +219,7 @@
     ring = [dev(zz=up), dev(zz=down)]
 
     barrier = pltpu.get_barrier_semaphore()
-    greet = others_y + others_zl + others_zg + others_tp + ring
+    greet = others_y + others_tp + ring
     for d in greet:
         pl.semaphore_signal(barrier, inc=1, device_id=d, device_id_type=MESH)
 
@@ -303,11 +303,19 @@
         ref = wo_rows(((x + NX - d) % NX) * NC + c)
         return rcopy(ref, ref, send.at[13], r_wo.at[NX - 1], partner)
 
+    def tell(i):
+        for zz in (z + 2**i, z + NZ - 2**i):
+            pl.semaphore_signal(ok.at[i], inc=1, device_id=dev(zz=zz % NZ), device_id_type=MESH)
+
+    def heard(i):
+        pl.semaphore_wait(ok.at[i], 2)
+
     def enter():
         for cp in loads[:3]:
             cp.wait()
         with jax.named_scope("enter"):
             pl.semaphore_wait(barrier, len(greet))
+        tell(0)
         for part in range(3):
             start(zstream(0, part, 0))
             start(yside(part, 0))
@@ -371,15 +379,18 @@
             with jax.named_scope("_".join([f.func.__name__] + [str(a) for a in f.args])):
                 f()
 
+    enter()
     for cp in loads[3:8]:
         cp.wait()
     with jax.named_scope("local"):
         prod, state, decay, outputs = local_part(
-            r_ref, k_ref, v_ref, dw_ref, lw_ref, enter
+            r_ref, k_ref, v_ref, dw_ref, lw_ref, lambda: serve(MID)
         )
         put_packet(ybuf, y, prod, state, decay)
     l1 = exchange(ybuf, y, r_l1, 14, others_y)
     start(l1)
+    heard(0)
+    tell(1)
     serve(SERVE[0])
     with jax.named_scope("local_out"):
         q, y_own = outputs()
@@ -412,6 +423,8 @@
         lax.fori_loop(0, count, step, 0)
 
     put_packet(zbuf, zl, *total(ybuf))
+    heard(1)
+    tell(2)
     l2 = exchange(zbuf, zl, r_l2, 15, others_zl)
     start(l2)
     with jax.named_scope("before_y"):
@@ -435,6 +448,7 @@
             for e in range(NY - 1)
         ]
 
+    heard(2)
     for d in range(1, NG):
         @pl.when(zg + d < NG)
         def _(d=d):
@@ -616,7 +630,8 @@
 LAG = 1
 GROUPS = ((0, 5), (5, 9), (9, 13), (13, 15), (15, 16))
 VMEM_MB = 58
-SERVE = (6, 1, 6, 9, 6, 9)
+MID = 1
+SERVE = (5, 4, 3, 9, 6, 9)
 TAIL = (0, 1)
 
 
@@ -669,6 +684,7 @@
             dma((len(GROUPS),)),
             dma((len(GROUPS),)),
             dma((14,)),
+            pltpu.SemaphoreType.REGULAR((3,)),
         ],
         compiler_params=pltpu.CompilerParams(
             collective_id=0, has_side_effects=True, vmem_limit_bytes=VMEM_MB * 1024 * 1024

time: 77.8 us -> 78.1 us (level)
  no operation moved by 1% of the time
where the time goes in v4:
time: 78.1 us; the launch traced here: 78 us
  Pallas kernels  77.3 us (99%)
    pallas_call x1, Pallas kernels, layer(): pl.pallas_call(layer_kernel, in_specs=[pl.BlockSpec(memory_space=pltpu.HB...  77.3 us

profile of v4, /device:TPU:1, one launch (start us, length us, event | category | flops | bytes accessed | tf_op | source)
XLA Modules:
  0.0 78.0 jit_solution(3856549832737332563)
XLA Ops:
  0.0 77.3 %layer.1 = f32[24,2048]{1,0:T(8,128)S(1)} custom-call(bf16[192,128]{1,0:T(8,128)(2,1)} %r_hbm.1, bf16[192,128]{1,0:T(8,128)(2,1)} %k_hbm.1, bf16[192,128]{1,0:T(8,128)(2,1)} %v_hbm.1, f32[192,128]{1,0:T(8,128)} %dw_hbm.1, f32[192,128]{1,0:T(8,128)} %lw_hbm.1, bf16[192,128]{1,0:T(8,128)(2,1)} %gate_hbm.1, f32[2,64]{1,0:T(2,128)} %tw_hbm.1, f32[1,128]{1,0:T(1,128)} %bitcast.5, ...), custom_call_target="tpu_custom_call" | custom-call | flops 3000000000 | bytes 8000000 | tf_op jit(solution)/shard_map/layer/pallas_call | solution.py:646
  77.3 0.7 convert_element_type.3

commit v5 on v4

--- a/solution.py
+++ b/solution.py
@@ -182,7 +182,7 @@
     out_ref,
     wall, wo, mixed, resid, after, normed, hid, parts, pair_in, pair_sum, last_in,
     r_ref, k_ref, v_ref, dw_ref, lw_ref, gate_ref, tw_ref, hg_ref, gain_ref,
-    ybuf, zbuf, gbuf, q_s, y_s, ent,
+    ybuf, zbuf, gbuf, q_s, y_s, ent, sums, acc,
     send, r_wo, r_z, r_q, r_y0, r_ya, r_yb, r_l1, r_l2, r_l3, x_l3, r_l4, x_l4, r_mx, r_pair, r_last, loc, ok,
 ):
     f32, bf16 = jnp.float32, jnp.bfloat16
@@ -259,7 +259,7 @@
             at = (0, depth) if s < HOPS - 1 else (half * d, half)
             ref = block(ahead(s, d), lane[st], part, *at)
             k = 3 * st + part
-            out.append(rcopy(ref, ref, send.at[k], r_z.at[k, s], ring[d]))
+            out.append(rcopy(ref, ref, send.at[0], r_z.at[k, s], ring[d]))
         return out
 
     side = [dev(yy=(y + 1) % NY), dev(yy=(y + NY - 1) % NY)]
@@ -267,16 +267,16 @@
     def yside(part, i):
         ref = block(plane_of(i), y, part)
         group = [g for g, (lo, hi) in enumerate(GROUPS) if lo <= i < hi][0]
-        sems = [r_ya.at[part] if part < DOWN else r_yb.at[group]] * 2
+        sems = [r_ya.at[2 * part + (i >= EARLY)] if part < DOWN else r_yb.at[group]] * 2
         if i == 0:
             sems = [r_y0.at[part]] * 2
-        return [rcopy(ref, ref, send.at[6 + part], sems[d], side[d]) for d in (0, 1)]
+        return [rcopy(ref, ref, send.at[0], sems[d], side[d]) for d in (0, 1)]
 
     def across(part):
         out = []
         for d in (0, 1):
             ref = block(z, (y + NY - 1) % NY if d == 0 else (y + 1) % NY, part, half * d, half)
-            out.append(rcopy(ref, ref, send.at[9 + part], r_q.at[part], side[d]))
+            out.append(rcopy(ref, ref, send.at[0], r_q.at[part], side[d]))
         return out
 
     def start(copies):
@@ -295,13 +295,13 @@
 
     def wo_same(d):
         t = ((x + d) % NX) * NC + c
-        return rcopy(wo_hbm, wo_rows(tp), send.at[12], r_wo.at[d - 1], dev(tt=t))
+        return rcopy(wo_hbm, wo_rows(tp), send.at[1], r_wo.at[d - 1], dev(tt=t))
 
     partner = dev(tt=x * NC + 1 - c)
 
     def wo_relay(d):
         ref = wo_rows(((x + NX - d) % NX) * NC + c)
-        return rcopy(ref, ref, send.at[13], r_wo.at[NX - 1], partner)
+        return rcopy(ref, ref, send.at[1], r_wo.at[NX - 1], partner)
 
     def tell(i):
         for zz in (z + 2**i, z + NZ - 2**i):
@@ -370,6 +370,7 @@
                     job(q_open, 1)
                     job(q_open, DOWN)
     a_last = [f for f in work if f.args[0] < DOWN and f.func is q_step][-1]
+    early = [f for f in work if f.func is q_step and f.args == (1, (EARLY - 2) // 2)][0]
     b_last = [f for f in work if f.args[0] == DOWN and f.func is q_step]
 
     def serve(n=None, until=None):
@@ -387,7 +388,7 @@
             r_ref, k_ref, v_ref, dw_ref, lw_ref, lambda: serve(MID)
         )
         put_packet(ybuf, y, prod, state, decay)
-    l1 = exchange(ybuf, y, r_l1, 14, others_y)
+    l1 = exchange(ybuf, y, r_l1, 2, others_y)
     start(l1)
     heard(0)
     tell(1)
@@ -425,7 +426,7 @@
     put_packet(zbuf, zl, *total(ybuf))
     heard(1)
     tell(2)
-    l2 = exchange(zbuf, zl, r_l2, 15, others_zl)
+    l2 = exchange(zbuf, zl, r_l2, 3, others_zl)
     start(l2)
     with jax.named_scope("before_y"):
         before(0, ybuf, y)
@@ -492,7 +493,7 @@
     yy = yy * lax.rsqrt(spread + GROUP_EPS) * hg_ref[...] + own
     mixed[tp] = (yy * jax.nn.sigmoid(gate_ref[...].astype(f32))).astype(bf16)
     mx = [
-        rcopy(mixed.at[tp], mixed.at[tp], send.at[17], r_mx.at[0], t)
+        rcopy(mixed.at[tp], mixed.at[tp], send.at[4], r_mx.at[0], t)
         for d, t in enumerate(others_tp)
     ]
     start(mx)
@@ -504,7 +505,7 @@
     wide = 512
 
     def project(n, ss):
-        cut = pl.ds(pl.multiple_of(n * wide, wide), wide)
+        cut = slice(n * wide, (n + 1) * wide)
         lhs = jnp.concatenate([mixed[j] for j in range(NTP)], axis=1)
         mix = jnp.dot(lhs, wo[:, cut], preferred_element_type=f32)
         mix = mix.astype(bf16).astype(f32)
@@ -512,8 +513,13 @@
         after[:, cut] = a
         return ss + jnp.sum(a * a, axis=-1, keepdims=True)
 
-    with jax.named_scope("project"):
-        ss = lax.fori_loop(0, model // wide, project, jnp.zeros((steps, 1), f32))
+    ss = jnp.zeros((steps, 1), f32)
+    for n in range(model // wide):
+        with jax.named_scope("project"):
+            ss = project(n, ss)
+            sums[...] = ss
+        serve(1)
+        ss = sums[...]
     factor = lax.rsqrt(ss * (1.0 / model) + NORM_EPS)
 
     def scale(n, _):
@@ -523,20 +529,41 @@
 
     with jax.named_scope("scale"):
         lax.fori_loop(0, model // wide, scale, 0)
+    def planes(lo, hi, part, at, n):
+        total = None
+        for i in range(lo, hi, 2):
+            pair = [plane_of(i), plane_of(i + 1)]
+            a = [normed[:, pl.ds(pl.multiple_of(p * plane, plane), plane)] for p in pair]
+            w = [wall[rows(p, 0, 0, plane), part * ff + at : part * ff + at + n] for p in pair]
+            d = jnp.dot(
+                jnp.concatenate(a, axis=1), jnp.concatenate(w, axis=0), preferred_element_type=f32
+            )
+            total = d if total is None else total + d
+        return total
+
+    chunks = [(at, min(256, ff - at)) for at in range(0, ff, 256)]
+    serve(until=early)
+    with jax.named_scope("wait_early"):
+        for part in range(DOWN):
+            wait_blocks(part, 2 * (EARLY - 1), r_ya.at[2 * part])
+    for at, n in chunks:
+        for part in range(DOWN):
+            with jax.named_scope("early"):
+                acc[:, part * ff + at : part * ff + at + n] = planes(0, EARLY, part, at, n)
+            serve(1)
     serve(until=a_last)
     serve(TAIL[0])
     with jax.named_scope("wait_gate_up"):
         for part in range(DOWN):
-            wait_bytes(wall.at[0 : 2 * (NZ - 1) * depth, cols[part]], r_ya.at[part])
+            wait_blocks(part, 2 * (NZ - EARLY), r_ya.at[2 * part + 1])
 
     with jax.named_scope("gate_up"):
-        lo = 0
-        while lo < ff:
-            n = min(256, ff - lo)
-            g = jnp.dot(normed[...], wall[:, lo : lo + n], preferred_element_type=f32)
-            u = jnp.dot(normed[...], wall[:, ff + lo : ff + lo + n], preferred_element_type=f32)
-            hid[:, lo : lo + n] = (g / (1.0 + jnp.exp(-g)) * u).astype(bf16)
-            lo += n
+        for at, n in chunks:
+            g, u = (
+                acc[:, part * ff + at : part * ff + at + n] + planes(EARLY, NZ, part, at, n)
+                for part in range(DOWN)
+            )
+            hid[:, at : at + n] = (g / (1.0 + jnp.exp(-g)) * u).astype(bf16)
 
     serve(TAIL[1])
 
@@ -553,7 +580,7 @@
     def pair(g):
         lo, hi = GROUPS[g]
         return rcopy(
-            parts.at[1 - c, lo:hi], pair_in.at[lo:hi], send.at[18], r_pair.at[g], partner
+            parts.at[1 - c, lo:hi], pair_in.at[lo:hi], send.at[5], r_pair.at[g], partner
         )
 
     def across_x(g):
@@ -563,7 +590,7 @@
             xx = (x + d) % NX
             out.append(
                 rcopy(
-                    pair_sum.at[xx, lo:hi], last_in.at[d - 1, lo:hi], send.at[19],
+                    pair_sum.at[xx, lo:hi], last_in.at[d - 1, lo:hi], send.at[6],
                     r_last.at[g], dev(tt=xx * NC + c),
                 )
             )
@@ -603,15 +630,10 @@
 
     drain = jax.named_scope("drain")
     drain.__enter__()
-    for k in range(6):
-        wait_bytes(wall.at[0 : (2 * HOPS - 1) * depth, cols[k % 3]], send.at[k])
-    for part in range(3):
-        wait_bytes(wall.at[0 : 2 * NZ * depth, cols[part]], send.at[6 + part])
-        wait_bytes(wall.at[0:depth, cols[part]], send.at[9 + part])
-    wait_bytes(wo.at[0 : (NX - 1) * LANES, :], send.at[12])
-    wait_bytes(wo.at[0 : NX * LANES, :], send.at[13])
-    wait_bytes(ybuf.at[0:3], send.at[14])
-    wait_bytes(zbuf.at[0:3], send.at[15])
+    wait_bytes(wall.at[0 : (2 * (2 * HOPS - 1) + 2 * NZ + 1) * depth, :], send.at[0])
+    wait_bytes(wo.at[0 : (2 * NX - 1) * LANES, :], send.at[1])
+    wait_bytes(ybuf.at[0:3], send.at[2])
+    wait_bytes(zbuf.at[0:3], send.at[3])
     for d in range(1, NG):
         @pl.when(zg + d < NG)
         def _(d=d):
@@ -620,18 +642,19 @@
         @pl.when(zg >= d)
         def _(d=d):
             wait_bytes(gbuf.at[0, 0 : LANES // NY * (NY - 1), :], x_l4.at[d - 1])
-    wait_bytes(mixed.at[0 : NTP - 1], send.at[17])
-    wait_bytes(pair_in, send.at[18])
-    wait_bytes(pair_sum.at[0 : NX - 1], send.at[19])
+    wait_bytes(mixed.at[0 : NTP - 1], send.at[4])
+    wait_bytes(pair_in, send.at[5])
+    wait_bytes(pair_sum.at[0 : NX - 1], send.at[6])
     drain.__exit__(None, None, None)
 
 
 DOWN = 2
+EARLY = 12
 LAG = 1
 GROUPS = ((0, 5), (5, 9), (9, 13), (13, 15), (15, 16))
 VMEM_MB = 58
 MID = 1
-SERVE = (5, 4, 3, 9, 6, 9)
+SERVE = (5, 4, 5, 7, 8, 10)
 TAIL = (0, 1)
 
 
@@ -667,12 +690,14 @@
             pltpu.VMEM((steps, LANES), f32),
             pltpu.VMEM((steps, LANES), f32),
             pltpu.VMEM((2, LANES, LANES), f32),
-            dma((20,)),
+            pltpu.VMEM((steps, 1), f32),
+            pltpu.VMEM((steps, 2 * ff), f32),
+            dma((7,)),
             dma((NX,)),
             dma((6, HOPS)),
             dma((3,)),
             dma((3,)),
-            dma((DOWN,)),
+            dma((2 * DOWN,)),
             dma((len(GROUPS),)),
             dma((1,)),
             dma((1,)),

time: 78.1 us -> 73.2 us (0.937)
  Pallas kernels: 77.3 us -> 72.5 us
    pallas_call x1, Pallas kernels: 77.3 us -> 72.5 us  [layer(): pl.pallas_call(layer_kernel, in_specs=[pl.BlockSpec(memory_space=pltpu.HB...]
where the time goes in v5:
time: 73.2 us; the launch traced here: 73.1 us
  Pallas kernels  72.5 us (99%)
    pallas_call x1, Pallas kernels, layer(): pl.pallas_call(layer_kernel, in_specs=[pl.BlockSpec(memory_space=pltpu.HB...  72.5 us

profile of v5, /device:TPU:1, one launch (start us, length us, event | category | flops | bytes accessed | tf_op | source)
XLA Modules:
  0.0 73.1 jit_solution(7183528389034115819)
XLA Ops:
  0.0 72.5 %layer.1 = f32[24,2048]{1,0:T(8,128)S(1)} custom-call(bf16[192,128]{1,0:T(8,128)(2,1)} %r_hbm.1, bf16[192,128]{1,0:T(8,128)(2,1)} %k_hbm.1, bf16[192,128]{1,0:T(8,128)(2,1)} %v_hbm.1, f32[192,128]{1,0:T(8,128)} %dw_hbm.1, f32[192,128]{1,0:T(8,128)} %lw_hbm.1, bf16[192,128]{1,0:T(8,128)(2,1)} %gate_hbm.1, f32[2,64]{1,0:T(2,128)} %tw_hbm.1, f32[1,128]{1,0:T(1,128)} %bitcast.5, ...), custom_call_target="tpu_custom_call" | custom-call | flops 3000000000 | bytes 8000000 | tf_op jit(solution)/shard_map/layer/pallas_call | solution.py:669
  72.5 0.7 convert_element_type.3

commit v6 on v5

--- a/solution.py
+++ b/solution.py
@@ -366,9 +366,8 @@
                 u = t - LAG if part == DOWN else t
                 if (0 if step is q_step else 1) <= u < HOPS:
                     job(step, part, u)
-                if s == 1 and step is p_step and part == 0:
-                    job(q_open, 1)
-                    job(q_open, DOWN)
+                if s == 1 and step is p_step and part < DOWN:
+                    job(q_open, part + 1)
     a_last = [f for f in work if f.args[0] < DOWN and f.func is q_step][-1]
     early = [f for f in work if f.func is q_step and f.args == (1, (EARLY - 2) // 2)][0]
     b_last = [f for f in work if f.args[0] == DOWN and f.func is q_step]
@@ -654,7 +653,7 @@
 GROUPS = ((0, 5), (5, 9), (9, 13), (13, 15), (15, 16))
 VMEM_MB = 58
 MID = 1
-SERVE = (5, 4, 5, 7, 8, 10)
+SERVE = (5, 5, 4, 7, 8, 10)
 TAIL = (0, 1)
 
 

time: 73.2 us -> 72.9 us (level)
  no operation moved by 1% of the time
where the time goes in v6:
time: 72.9 us; the launch traced here: 72.7 us
  Pallas kernels  72.1 us (99%)
    pallas_call x1, Pallas kernels, layer(): pl.pallas_call(layer_kernel, in_specs=[pl.BlockSpec(memory_space=pltpu.HB...  72.1 us

profile of v6, /device:TPU:1, one launch (start us, length us, event | category | flops | bytes accessed | tf_op | source)
XLA Modules:
  0.0 72.7 jit_solution(2267370779363595078)
XLA Ops:
  0.0 72.1 %layer.1 = f32[24,2048]{1,0:T(8,128)S(1)} custom-call(bf16[192,128]{1,0:T(8,128)(2,1)} %r_hbm.1, bf16[192,128]{1,0:T(8,128)(2,1)} %k_hbm.1, bf16[192,128]{1,0:T(8,128)(2,1)} %v_hbm.1, f32[192,128]{1,0:T(8,128)} %dw_hbm.1, f32[192,128]{1,0:T(8,128)} %lw_hbm.1, bf16[192,128]{1,0:T(8,128)(2,1)} %gate_hbm.1, f32[2,64]{1,0:T(2,128)} %tw_hbm.1, f32[1,128]{1,0:T(1,128)} %bitcast.5, ...), custom_call_target="tpu_custom_call" | custom-call | flops 3000000000 | bytes 8000000 | tf_op jit(solution)/shard_map/layer/pallas_call | solution.py:668
  72.1 0.7 convert_element_type.3

commit v7 on v6

--- a/solution.py
+++ b/solution.py
@@ -650,7 +650,7 @@
 DOWN = 2
 EARLY = 12
 LAG = 1
-GROUPS = ((0, 5), (5, 9), (9, 13), (13, 15), (15, 16))
+GROUPS = ((0, 3), (3, 7), (7, 11), (11, 15), (15, 16))
 VMEM_MB = 58
 MID = 1
 SERVE = (5, 5, 4, 7, 8, 10)

time: 72.9 us -> 72.8 us (level)
  no operation moved by 1% of the time
where the time goes in v7:
time: 72.8 us; the launch traced here: 72.7 us
  Pallas kernels  72 us (99%)
    pallas_call x1, Pallas kernels, layer(): pl.pallas_call(layer_kernel, in_specs=[pl.BlockSpec(memory_space=pltpu.HB...  72 us

profile of v7, /device:TPU:1, one launch (start us, length us, event | category | flops | bytes accessed | tf_op | source)
XLA Modules:
  0.0 72.7 jit_solution(277684918983628254)
XLA Ops:
  0.0 72.0 %layer.1 = f32[24,2048]{1,0:T(8,128)S(1)} custom-call(bf16[192,128]{1,0:T(8,128)(2,1)} %r_hbm.1, bf16[192,128]{1,0:T(8,128)(2,1)} %k_hbm.1, bf16[192,128]{1,0:T(8,128)(2,1)} %v_hbm.1, f32[192,128]{1,0:T(8,128)} %dw_hbm.1, f32[192,128]{1,0:T(8,128)} %lw_hbm.1, bf16[192,128]{1,0:T(8,128)(2,1)} %gate_hbm.1, f32[2,64]{1,0:T(2,128)} %tw_hbm.1, f32[1,128]{1,0:T(1,128)} %bitcast.5, ...), custom_call_target="tpu_custom_call" | custom-call | flops 3000000000 | bytes 8000000 | tf_op jit(solution)/shard_map/layer/pallas_call | solution.py:668
  72.0 0.7 convert_element_type.3
